TPU v7x, 32 devices: a whole 2x2x4 slice. The times are simulated.
32 devices in a mesh: sp: 4 (over y, x), tp: 8 (over z, core).
Axes of the slice: x: 2, y: 2, z: 4, core: 2. Of those that a mesh axis runs over, the one named last changes fastest.
Arguments:
- tokens: bfloat16 [2, 512, 4096], P(None, 'sp', 'tp'), may hold values from -6 to 6
- key_matrix: bfloat16 [4096, 4096], P(None, 'tp'), may hold values from -0.09375 to 0.09375
- value_matrix: bfloat16 [4096, 4096], P(None, 'tp'), may hold values from -0.375 to 0.375
- gate_matrix: bfloat16 [4096, 64], replicated, may hold values from -0.09375 to 0.09375
- head_decay_rate: float32 [32], P('tp'), may hold values from 0 to 1, as said below
- extra_log_decay: float32 [2, 32, 512], P(None, 'tp', 'sp'), may hold values from -3 to 0, as said below
- next_token_query: bfloat16 [2, 4096], P(None, 'tp'), may hold values from -6 to 6
- next_token_key: bfloat16 [2, 4096], P(None, 'tp'), may hold values from -6 to 6
- next_token_value: bfloat16 [2, 32, 128], P(None, 'tp', 'sp'), may hold values from -6 to 6
- next_write_strength: float32 [2, 32], P(None, 'tp'), may hold values from 0.05 to 1
- read_norm_gain: float32 [128], P('sp'), may hold values from 0.1 to 1.9
Outputs:
- state_cache: bfloat16 [2, 32, 128, 128], P(None, 'tp', None, 'sp')
- first_read: bfloat16 [2, 32, 128], P(None, 'tp', 'sp')
Inputs may be any that keep to these rules, and one draw needn't show every extreme that they name: `head_decay_rate`: positive. `extra_log_decay`: never positive.
All inputs are finite; a program needn't handle non-finite values.
Results may differ from a plain program's by a relative error of at most 0.013.
Values may be sent and summed in bfloat16 or wider, within the bound.
A program may use at most 64 MiB of HBM per device.

v0:
```python
import functools

import jax
import jax.numpy as jnp
from jax import lax
from jax.experimental import pallas as pl
from jax.experimental.pallas import tpu as pltpu
from jax.sharding import PartitionSpec as P

DV = 128
CORES = 2
MESH = pl.DeviceIdType.MESH


exact_mode = lax.Precision.HIGHEST
strength_offset = 5.0


def unit_rows(matrix):
    return matrix * lax.rsqrt(jnp.sum(matrix * matrix, axis=-1, keepdims=True) + 1e-06)


def nilpotent_inverse(mixing):
    extent = mixing.shape[-1]
    result = jnp.zeros_like(mixing) + jnp.eye(extent, dtype=jnp.float32)
    powered = -mixing
    covered = 1
    while covered < extent:
        product = lax.optimization_barrier(
            jnp.einsum("...ij,...jk->...ik", result, powered, precision=exact_mode)
        )
        result = result + product
        powered = jnp.einsum("...ij,...jk->...ik", powered, powered, precision=exact_mode)
        covered = covered * 2
    return result


def block_terms(unit_keys, values, decay_logarithm, strength):
    extent = unit_keys.shape[-2]
    lower = jnp.tril(jnp.ones((extent, extent), jnp.bool_))
    strict = jnp.tril(jnp.ones((extent, extent), jnp.bool_), -1)
    running = jnp.cumsum(decay_logarithm, axis=-1)
    spread = running[..., :, None] - running[..., None, :]
    within = jnp.where(lower, jnp.exp(jnp.where(lower, spread, 0.0)), 0.0)
    scaled = unit_keys * strength[..., None]
    mixing = jnp.where(
        strict,
        jnp.einsum("...id,...jd->...ij", scaled, unit_keys, precision=exact_mode) * within,
        0.0,
    )
    inverse = nilpotent_inverse(mixing)
    writes = jnp.einsum(
        "...ij,...je->...ie", inverse, values * strength[..., None], precision=exact_mode
    )
    erases = jnp.einsum(
        "...ij,...jd->...id", inverse, scaled * jnp.exp(running)[..., None], precision=exact_mode
    )
    final_log = running[..., -1]
    carried = unit_keys * jnp.exp(final_log[..., None] - running)[..., None]
    return (writes, erases, carried, final_log)


def split_blocks(array, block_count):
    shaped = array.reshape(
        array.shape[:2] + (block_count, array.shape[2] // block_count) + array.shape[3:]
    )
    return jnp.moveaxis(shaped, 2, 0)


def local_general(
    tokens,
    key_matrix,
    value_matrix,
    gate_matrix,
    head_decay_rate,
    extra_log_decay,
    next_token_query,
    next_token_key,
    next_token_value,
    next_write_strength,
    read_norm_gain,
):
    sequences, positions, _ = tokens.shape
    local_heads = head_decay_rate.shape[0]
    key_width = key_matrix.shape[1] // local_heads
    value_width = value_matrix.shape[1] // local_heads
    all_heads = gate_matrix.shape[1] // 2
    group_size = lax.axis_size("sp")
    column_share = value_width // group_size
    first_head = lax.axis_index("tp") * local_heads
    decay_cols = lax.dynamic_slice_in_dim(gate_matrix, first_head, local_heads, 1)
    strength_cols = lax.dynamic_slice_in_dim(gate_matrix, all_heads + first_head, local_heads, 1)
    gate_cols = jnp.concatenate([decay_cols, strength_cols], axis=1)
    row_count = sequences * positions
    incoming = lax.all_gather(tokens, "tp", axis=2, tiled=True)
    span_width = incoming.shape[2]
    flat_rows = incoming.reshape(row_count, span_width)
    products = lax.optimization_barrier(
        (
            jnp.dot(flat_rows, key_matrix, preferred_element_type=jnp.float32),
            jnp.dot(flat_rows, value_matrix, preferred_element_type=jnp.float32),
            jnp.dot(flat_rows, gate_cols, preferred_element_type=jnp.float32),
        )
    )
    key_sum = products[0]
    value_sum = products[1]
    gate_pre = products[2]
    key_float = lax.optimization_barrier(key_sum.astype(jnp.bfloat16)).astype(jnp.float32)
    value_float = lax.optimization_barrier(value_sum.astype(jnp.bfloat16)).astype(jnp.float32)
    unit_keys = unit_rows(
        key_float.reshape(sequences, positions, local_heads, key_width).transpose(0, 2, 1, 3)
    )
    values = value_float.reshape(sequences, positions, local_heads, value_width).transpose(
        0, 2, 1, 3
    )
    gate_projected = gate_pre.reshape(sequences, positions, 2 * local_heads).transpose(0, 2, 1)
    decay_logarithm = (
        -head_decay_rate[None, :, None] * jax.nn.softplus(gate_projected[:, :local_heads])
        + extra_log_decay
    )
    strength = jax.nn.sigmoid(gate_projected[:, local_heads:] - strength_offset)
    block_count = positions // min(64, positions)
    block_parts = block_terms(
        split_blocks(unit_keys, block_count),
        split_blocks(values, block_count),
        split_blocks(decay_logarithm, block_count),
        split_blocks(strength, block_count),
    )
    identity = jnp.zeros((sequences, local_heads, key_width, key_width), jnp.float32) + jnp.eye(
        key_width, dtype=jnp.float32
    )
    start_map = jnp.concatenate(
        [identity, jnp.zeros((sequences, local_heads, key_width, value_width), jnp.float32)],
        axis=-1,
    )

    def advance(current, block_part):
        writes, erases, carried, final_log = block_part
        padded = jnp.concatenate(
            [jnp.zeros(writes.shape[:-1] + (key_width,), jnp.float32), writes], axis=-1
        )
        removed = lax.optimization_barrier(
            jnp.einsum("shcd,shde->shce", erases, current, precision=exact_mode)
        )
        fresh = padded - removed
        added = lax.optimization_barrier(
            jnp.einsum("shcd,shce->shde", carried, fresh, precision=exact_mode)
        )
        current = current * jnp.exp(final_log)[..., None, None] + added
        return (current, None)

    local_map, _ = lax.scan(advance, start_map, block_parts)
    carry_map = local_map[..., :key_width]
    write_map = local_map[..., key_width:]
    carry_copies = jnp.broadcast_to(carry_map[None], (group_size,) + carry_map.shape)
    write_parts = jnp.moveaxis(
        write_map.reshape(sequences, local_heads, key_width, group_size, column_share), 3, 0
    )
    carries = lax.all_to_all(carry_copies, "sp", split_axis=0, concat_axis=0, tiled=True)
    write_cols = lax.all_to_all(write_parts, "sp", split_axis=0, concat_axis=0, tiled=True)

    def fold_step(current, block_map):
        moved = lax.optimization_barrier(
            jnp.einsum("shij,shje->shie", block_map[0], current, precision=exact_mode)
        )
        return (moved + block_map[1], None)

    begin_state = jnp.zeros(write_cols.shape[1:], jnp.float32)
    folded, _ = lax.scan(fold_step, begin_state, (carries, write_cols))
    query_rows = next_token_query.astype(jnp.float32).reshape(sequences, local_heads, key_width)
    unit_new = unit_rows(
        next_token_key.astype(jnp.float32).reshape(sequences, local_heads, key_width)
    )
    value_rows = next_token_value.astype(jnp.float32)
    key_read = jnp.einsum("shd,shde->she", unit_new, folded, precision=exact_mode)
    query_read = jnp.einsum("shd,shde->she", query_rows, folded, precision=exact_mode)
    intersection = jnp.sum(query_rows * unit_new, axis=-1)
    read_raw = query_read + (next_write_strength * intersection)[..., None] * (
        value_rows - key_read
    )
    square_total = lax.psum(jnp.sum(read_raw * read_raw, axis=-1, keepdims=True), "sp")
    first_read = read_raw * lax.rsqrt(square_total / DV + 1e-06) * read_norm_gain
    return (folded.astype(jnp.bfloat16), first_read.astype(jnp.bfloat16))


def exact_dot(left, right, contract=((1,), (0,))):
    return lax.dot_general(
        left, right, (contract, ((), ())), precision=exact_mode, preferred_element_type=jnp.float32
    )


def short_dot(left, right, contract=((1,), (0,))):
    return lax.dot_general(
        left.astype(jnp.bfloat16),
        right.astype(jnp.bfloat16),
        (contract, ((), ())),
        preferred_element_type=jnp.float32,
    )


def softplus(x):
    return jnp.maximum(x, 0.0) + jnp.log1p(jnp.exp(-jnp.abs(x)))


def grid_mask(rows, cols, rule):
    row = lax.broadcasted_iota(jnp.int32, (rows, cols), 0)
    col = lax.broadcasted_iota(jnp.int32, (rows, cols), 1)
    return rule(row, col)


def fused_kernel(
    sp_size,
    tp_size,
    rate_ref,
    next_strength_ref,
    tokens_ref,
    key_ref,
    value_ref,
    gate_hbm,
    extra_hbm,
    query_hbm,
    new_key_hbm,
    new_value_hbm,
    gain_hbm,
    state_ref,
    read_ref,
    gathered,
    key_w,
    value_w,
    gate_ref,
    extra_ref,
    query_ref,
    new_key_ref,
    new_value_ref,
    gain_ref,
    key_acc,
    value_acc,
    gate_acc,
    kv_out,
    kv_in,
    side_out,
    side_in,
    state_out,
    state_in,
    row_out,
    row_in,
    load_sem,
    weight_sem,
    gather_recv,
    gather_send,
    swap_recv,
    swap_send,
    swap_local,
    last_recv,
    last_send,
    last_local,
):
    sequences, positions, depth = tokens_ref.shape
    local_heads = extra_ref.shape[1]
    key_width = key_acc.shape[1] // local_heads
    value_width = value_acc.shape[1] // local_heads
    share = value_width // sp_size
    all_heads = gate_ref.shape[0] // 2
    chips = tp_size // CORES
    me = lax.axis_index("sp")
    spot = lax.axis_index("tp")
    chip = spot // CORES
    core = spot % CORES
    partner = chip * CORES + (1 - core)

    loads = [
        pltpu.make_async_copy(tokens_ref.at[s], gathered.at[spot, s], load_sem.at[s])
        for s in range(sequences)
    ]
    for load in loads:
        load.start()

    barrier = pltpu.get_barrier_semaphore()
    pl.semaphore_signal(barrier, inc=1, device_id={"tp": partner}, device_id_type=MESH)

    @pl.when(chip > 0)
    def _():
        pl.semaphore_signal(barrier, inc=1, device_id={"tp": spot - CORES}, device_id_type=MESH)

    @pl.when(chip < chips - 1)
    def _():
        pl.semaphore_signal(barrier, inc=1, device_id={"tp": spot + CORES}, device_id_type=MESH)

    for offset in range(1, sp_size):
        pl.semaphore_signal(
            barrier, inc=1, device_id={"sp": (me + offset) % sp_size}, device_id_type=MESH
        )
    weights = [
        pltpu.make_async_copy(key_ref, key_w, weight_sem.at[0]),
        pltpu.make_async_copy(value_ref, value_w, weight_sem.at[1]),
        pltpu.make_async_copy(gate_hbm, gate_ref, weight_sem.at[2]),
        pltpu.make_async_copy(extra_hbm, extra_ref, weight_sem.at[3]),
        pltpu.make_async_copy(query_hbm, query_ref, weight_sem.at[4]),
        pltpu.make_async_copy(new_key_hbm, new_key_ref, weight_sem.at[5]),
        pltpu.make_async_copy(new_value_hbm, new_value_ref, weight_sem.at[6]),
        pltpu.make_async_copy(gain_hbm, gain_ref, weight_sem.at[7]),
    ]
    for weight in weights:
        weight.start()
    key_acc[...] = jnp.zeros_like(key_acc)
    value_acc[...] = jnp.zeros_like(value_acc)
    gate_acc[...] = jnp.zeros_like(gate_acc)
    side_out[...] = jnp.zeros_like(side_out)
    row_out[...] = jnp.zeros_like(row_out)
    for load in loads:
        load.wait()
    near = jnp.where(chip > 0, 1, 0) + jnp.where(chip < chips - 1, 1, 0)
    pl.semaphore_wait(barrier, near + sp_size)

    def piece(origin, s, way, target):
        return pltpu.make_async_remote_copy(
            src_ref=gathered.at[origin, s],
            dst_ref=gathered.at[origin, s],
            send_sem=gather_send.at[origin, s, way],
            recv_sem=gather_recv.at[origin, s],
            device_id={"tp": target},
            device_id_type=MESH,
        )

    def take(block, s):
        rows = gathered[block, s]
        cut = slice(s * positions, (s + 1) * positions)
        span = pl.ds(pl.multiple_of(block * depth, depth), depth)
        key_acc[cut] += jnp.dot(rows, key_w[span, :], preferred_element_type=jnp.float32)
        value_acc[cut] += jnp.dot(rows, value_w[span, :], preferred_element_type=jnp.float32)
        gate_acc[cut] += lax.dot_general(
            rows,
            gate_ref[:, span],
            (((1,), (1,)), ((), ())),
            preferred_element_type=jnp.float32,
        )

    first = spot * local_heads
    chooser = grid_mask(
        2 * local_heads,
        2 * all_heads,
        lambda r, c: c == jnp.where(r < local_heads, first + r, all_heads + first + r - local_heads),
    ).astype(jnp.float32)
    placer = grid_mask(share, value_width, lambda r, c: c == me * share + r).astype(jnp.float32)

    def swap(s, target, origin):
        return [
            pltpu.make_async_remote_copy(
                src_ref=source.at[target, s],
                dst_ref=sink.at[origin, s],
                send_sem=swap_send.at[n, s, target],
                recv_sem=swap_recv.at[n, s, origin],
                device_id={"sp": target},
                device_id_type=MESH,
            )
            for n, (source, sink) in enumerate(((side_out, side_in), (kv_out, kv_in)))
        ]

    def kept(s):
        return [
            pltpu.make_async_copy(kv_out.at[me, s], kv_in.at[me, s], swap_local.at[0, s]),
            pltpu.make_async_copy(side_out.at[me, s], side_in.at[me, s], swap_local.at[1, s]),
        ]

    def hand_out(s):
        cut = slice(s * positions, (s + 1) * positions)
        gates = exact_dot(chooser, gate_acc[cut], ((1,), (1,)))
        new_value = exact_dot(new_value_ref[s].astype(jnp.float32), placer)
        extra = extra_ref[s]
        for h in range(local_heads):
            kv_out[h, s, 0] = key_acc[cut, h * key_width : (h + 1) * key_width].astype(jnp.bfloat16)
            kv_out[h, s, 1] = value_acc[cut, h * value_width : (h + 1) * value_width].astype(
                jnp.bfloat16
            )
            side_out[h, s, 0:1, :] = (
                -rate_ref[h] * softplus(gates[h : h + 1]) + extra[h : h + 1, :]
            )
            side_out[h, s, 1:2, :] = jax.nn.sigmoid(
                gates[local_heads + h : local_heads + h + 1] - strength_offset
            )
            side_out[h, s, 2:3, :] = new_value[h : h + 1, :]
        for n in range(2):
            for offset in range(1, sp_size):
                swap(s, (me + offset) % sp_size, me)[n].start()
        for copy in kept(s):
            copy.start()

    for s in range(sequences):

        @pl.when(chip < chips - 1)
        def _(s=s):
            piece(spot, s, 0, spot + CORES).start()

        @pl.when(chip > 0)
        def _(s=s):
            piece(spot, s, 1, spot - CORES).start()

        piece(spot, s, 2, partner).start()
    for weight in weights:
        weight.wait()
    for s in range(sequences):
        take(spot, s)
        piece(partner, s, 2, partner).wait_recv()
        take(partner, s)

    for distance in range(1, chips):
        for s in range(sequences):
            for way, step in ((0, -1), (1, 1)):
                origin_chip = chip + step * distance
                origin = origin_chip * CORES + core
                present = (origin_chip >= 0) & (origin_chip < chips)
                onward = chip - step

                @pl.when(present)
                def _(s=s, way=way, origin=origin, onward=onward):
                    piece(origin, s, way, partner).wait_recv()

                    @pl.when((onward >= 0) & (onward < chips))
                    def _():
                        piece(origin, s, way, onward * CORES + core).start()

                    piece(origin, s, 2, partner).start()

            def absorb(index, carry, distance=distance, s=s):
                side = index // CORES
                which = index % CORES
                origin_chip = chip + (2 * side - 1) * distance
                present = (origin_chip >= 0) & (origin_chip < chips)

                @pl.when(present & (which == 0))
                def _():
                    take(origin_chip * CORES + core, s)

                @pl.when(present & (which == 1))
                def _():
                    block = origin_chip * CORES + 1 - core
                    piece(block, s, 2, partner).wait_recv()
                    take(block, s)

                return carry

            lax.fori_loop(0, 2 * CORES, absorb, 0)
            if distance == chips - 1:
                hand_out(s)

    side_rows = side_in.shape[2]
    upto = grid_mask(positions, positions, lambda r, c: r <= c).astype(jnp.float32)
    eye = grid_mask(positions, positions, lambda r, c: r == c).astype(jnp.float32)
    lower = grid_mask(positions, positions, lambda r, c: r >= c)
    strict = grid_mask(positions, positions, lambda r, c: r > c)
    lanes = pl.ds(pl.multiple_of(me * key_width, key_width), key_width)
    queries = query_ref[:, lanes].astype(jnp.float32)
    new_keys = new_key_ref[:, lanes].astype(jnp.float32)
    new_keys = new_keys * lax.rsqrt(jnp.sum(new_keys * new_keys, axis=-1, keepdims=True) + 1e-06)
    meets = jnp.sum(queries * new_keys, axis=-1, keepdims=True)

    def final(n, s, source, sink, target, origin):
        return pltpu.make_async_remote_copy(
            src_ref=source,
            dst_ref=sink.at[origin, s],
            send_sem=last_send.at[n, s, target],
            recv_sem=last_recv.at[n, s, origin],
            device_id={"sp": target},
            device_id_type=MESH,
        )

    def stay(s):
        return [
            pltpu.make_async_copy(state_out.at[me, s], state_in.at[me, s], last_local.at[0, s]),
            pltpu.make_async_copy(row_out.at[s], row_in.at[me, s], last_local.at[1, s]),
        ]

    for s in range(sequences):
        for copy in kept(s):
            copy.wait()
        for offset in range(1, sp_size):
            source = (me + offset) % sp_size
            swap(s, source, source)[0].wait_recv()
        side = side_in[:, s].reshape(sp_size * side_rows, positions)
        running_row = exact_dot(side, upto)
        running_col = exact_dot(upto, side, ((0,), (1,)))
        side_col = exact_dot(eye, side, ((1,), (1,)))
        for offset in range(1, sp_size):
            source = (me + offset) % sp_size
            swap(s, source, source)[1].wait_recv()
        parts = []
        for b in range(sp_size):
            line = b * side_rows
            row = running_row[line : line + 1, :]
            col = running_col[:, line : line + 1]
            strength = side_col[:, line + 1 : line + 2]
            final_log = row[:, positions - 1 : positions]
            keys = kv_in[b, s, 0].astype(jnp.float32)
            keys = keys * lax.rsqrt(jnp.sum(keys * keys, axis=-1, keepdims=True) + 1e-06)
            within = jnp.where(lower, jnp.exp(jnp.where(lower, col - row, 0.0)), 0.0)
            scaled = keys * strength
            power = jnp.where(strict, -short_dot(scaled, keys, ((1,), (1,))) * within, 0.0)
            targets = jnp.concatenate(
                [kv_in[b, s, 1].astype(jnp.float32) * strength, scaled * jnp.exp(col)], axis=1
            ).astype(jnp.bfloat16)
            carried = (keys * jnp.exp(final_log - col)).T.astype(jnp.bfloat16)
            parts.append([eye + power, power, targets, carried, jnp.exp(final_log)])
        for part in parts:
            part[1] = short_dot(part[1], part[1])
        covered = 2
        while covered < positions:
            for part in parts:
                if covered * 2 < positions:
                    both = short_dot(part[1], jnp.concatenate([part[0], part[1]], axis=1))
                    part[0] = part[0] + both[:, :positions]
                    part[1] = both[:, positions:]
                else:
                    part[0] = part[0] + short_dot(part[1], part[0])
            covered = covered * 2
        for part in parts:
            part[2] = short_dot(part[0], part[2])
        state = None
        for _, _, solved, carried, shrink in parts:
            fresh = solved[:, :value_width]
            if state is None:
                state = short_dot(carried, fresh)
            else:
                fresh = fresh - short_dot(solved[:, value_width:], state)
                state = state * shrink + short_dot(carried, fresh)

        turned = state.T.astype(jnp.bfloat16)
        for j in range(sp_size):
            state_out[j, s] = turned[j * share : (j + 1) * share, :]
        for offset in range(1, sp_size):
            target = (me + offset) % sp_size
            final(0, s, state_out.at[target, s], state_in, target, me).start()
        wide = (8, key_width)
        first_row = grid_mask(*wide, lambda r, c: r == 0)
        probes = jnp.where(
            first_row,
            jnp.broadcast_to(queries[s : s + 1], wide),
            jnp.broadcast_to(new_keys[s : s + 1], wide),
        )
        reads = exact_dot(probes, state)
        query_read, key_read = reads[0:1], reads[1:2]
        new_value = jnp.sum(side_in[:, s, 2, :], axis=0, keepdims=True)
        raw = query_read + (next_strength_ref[s, me] * meets[s : s + 1]) * (new_value - key_read)
        row_out[s, 0:1, :] = raw * lax.rsqrt(
            jnp.sum(raw * raw, axis=-1, keepdims=True) / value_width + 1e-06
        )
        for offset in range(1, sp_size):
            target = (me + offset) % sp_size
            final(1, s, row_out.at[s], row_in, target, me).start()
        for copy in stay(s):
            copy.start()

    picker = grid_mask(value_width, share, lambda r, c: r == me * share + c).astype(jnp.float32)
    row_lines = row_in.shape[2]
    for s in range(sequences):
        for copy in stay(s):
            copy.wait()
        for offset in range(1, sp_size):
            source = (me + offset) % sp_size
            final(0, s, state_in.at[source, s], state_in, source, source).wait_recv()
            final(1, s, row_in.at[source, s], row_in, source, source).wait_recv()
        rows = exact_dot(row_in[:, s].reshape(sp_size * row_lines, value_width), picker)
        rows = rows * gain_ref[...].reshape(1, share)
        read_ref[s] = jnp.concatenate(
            [rows[i * row_lines : i * row_lines + 1] for i in range(sp_size)], axis=0
        ).astype(jnp.bfloat16)
        for i in range(sp_size):
            state_ref[s, i] = state_in[i, s]

    for s in range(sequences):
        for offset in range(1, sp_size):
            target = (me + offset) % sp_size
            for copy in swap(s, target, me):
                copy.wait_send()
            final(0, s, state_out.at[target, s], state_in, target, me).wait_send()
            final(1, s, row_out.at[s], row_in, target, me).wait_send()
    for distance in range(chips):
        for way, step in ((0, -1), (1, 1)):
            if distance == 0 and way == 1:
                continue
            origin_chip = chip + step * distance
            origin = origin_chip * CORES + core

            @pl.when((origin_chip >= 0) & (origin_chip < chips))
            def _(origin=origin):
                for s in range(sequences):
                    piece(origin, s, 2, partner).wait_send()

            for other, onward in ((0, chip + 1), (1, chip - 1)):
                if distance and other != way:
                    continue

                @pl.when(
                    (origin_chip >= 0)
                    & (origin_chip < chips)
                    & (onward >= 0)
                    & (onward < chips)
                )
                def _(origin=origin, other=other, onward=onward):
                    for s in range(sequences):
                        piece(origin, s, other, onward * CORES + core).wait_send()


def local_fused(
    tokens,
    key_matrix,
    value_matrix,
    gate_matrix,
    head_decay_rate,
    extra_log_decay,
    next_token_query,
    next_token_key,
    next_token_value,
    next_write_strength,
    read_norm_gain,
):
    sequences, positions, depth = tokens.shape
    local_heads = head_decay_rate.shape[0]
    sp_size = lax.axis_size("sp")
    tp_size = lax.axis_size("tp")
    key_total = key_matrix.shape[1]
    value_total = value_matrix.shape[1]
    key_width = key_total // local_heads
    value_width = value_total // local_heads
    share = value_width // sp_size
    rows = sequences * positions
    vmem = pl.BlockSpec(memory_space=pltpu.VMEM)
    smem = pl.BlockSpec(memory_space=pltpu.SMEM)
    anywhere = pl.BlockSpec(memory_space=pl.ANY)
    dma = pltpu.SemaphoreType.DMA
    turned, read = pl.pallas_call(
        functools.partial(fused_kernel, sp_size, tp_size),
        out_shape=(
            jax.ShapeDtypeStruct((sequences, local_heads, share, key_width), jnp.bfloat16),
            jax.ShapeDtypeStruct((sequences, local_heads, share), jnp.bfloat16),
        ),
        in_specs=[smem, smem] + [anywhere] * 9,
        out_specs=(vmem, vmem),
        scratch_shapes=[
            pltpu.VMEM((tp_size, sequences, positions, depth), jnp.bfloat16),
            pltpu.VMEM(key_matrix.shape, jnp.bfloat16),
            pltpu.VMEM(value_matrix.shape, jnp.bfloat16),
            pltpu.VMEM(gate_matrix.shape[::-1], jnp.bfloat16),
            pltpu.VMEM(extra_log_decay.shape, jnp.float32),
            pltpu.VMEM(next_token_query.shape, jnp.bfloat16),
            pltpu.VMEM(next_token_key.shape, jnp.bfloat16),
            pltpu.VMEM(next_token_value.shape, jnp.bfloat16),
            pltpu.VMEM(read_norm_gain.shape, jnp.float32),
            pltpu.VMEM((rows, key_total), jnp.float32),
            pltpu.VMEM((rows, value_total), jnp.float32),
            pltpu.VMEM((rows, gate_matrix.shape[1]), jnp.float32),
            pltpu.VMEM((sp_size, sequences, 2, positions, key_width), jnp.bfloat16),
            pltpu.VMEM((sp_size, sequences, 2, positions, key_width), jnp.bfloat16),
            pltpu.VMEM((sp_size, sequences, 8, positions), jnp.float32),
            pltpu.VMEM((sp_size, sequences, 8, positions), jnp.float32),
            pltpu.VMEM((sp_size, sequences, share, key_width), jnp.bfloat16),
            pltpu.VMEM((sp_size, sequences, share, key_width), jnp.bfloat16),
            pltpu.VMEM((sequences, 8, value_width), jnp.float32),
            pltpu.VMEM((sp_size, sequences, 8, value_width), jnp.float32),
            dma((sequences,)),
            dma((8,)),
            dma((tp_size, sequences)),
            dma((tp_size, sequences, 3)),
            dma((2, sequences, sp_size)),
            dma((2, sequences, sp_size)),
            dma((2, sequences)),
            dma((2, sequences, sp_size)),
            dma((2, sequences, sp_size)),
            dma((2, sequences)),
        ],
        compiler_params=pltpu.CompilerParams(
            collective_id=0, has_side_effects=True
        ),
    )(
        head_decay_rate,
        next_write_strength,
        tokens,
        key_matrix,
        value_matrix,
        gate_matrix.T,
        extra_log_decay,
        next_token_query,
        next_token_key,
        next_token_value,
        read_norm_gain,
    )
    return jnp.swapaxes(turned, 2, 3), read


def local(*arguments):
    tokens, key_matrix, value_matrix = arguments[:3]
    sequences, positions, _ = tokens.shape
    local_heads = arguments[4].shape[0]
    sp_size = lax.axis_size("sp")
    fits = (
        local_heads == sp_size
        and sequences == 2
        and lax.axis_size("tp") % CORES == 0
        and lax.axis_size("tp") > CORES
        and positions == key_matrix.shape[1] // local_heads
        and positions == value_matrix.shape[1] // local_heads
        and positions % 128 == 0
    )
    return local_fused(*arguments) if fits else local_general(*arguments)


def solution(mesh):
    in_specs = (
        P(None, "sp", "tp"),
        P(None, "tp"),
        P(None, "tp"),
        P(),
        P("tp"),
        P(None, "tp", "sp"),
        P(None, "tp"),
        P(None, "tp"),
        P(None, "tp", "sp"),
        P(None, "tp"),
        P("sp"),
    )
    out_specs = (P(None, "tp", None, "sp"), P(None, "tp", "sp"))
    return jax.shard_map(local, mesh=mesh, in_specs=in_specs, out_specs=out_specs, check_vma=False)
```

profile of v0, /device:TPU:0, one launch (start us, length us, event | category | flops | bytes accessed | tf_op | source)
XLA Modules:
  0.0 42.7 jit_solution(9719492716582711447)
XLA Ops:
  0.6 39.3 %shard_map.122 = (bf16[2,4,32,128]{3,2,1,0:T(8,128)(2,1)}, bf16[2,4,32]{2,1,0:T(4,128)(2,1)}) custom-call(f32[4]{0:T(128)} %rate_ref.1, f32[2,4]{1,0:T(2,128)} %next_strength_ref.1, bf16[2,128,512]{2,1,0:T(8,128)(2,1)} %tokens_ref.1, bf16[4096,512]{1,0:T(8,128)(2,1)} %key_ref.1, bf16[4096,512]{1,0:T(8,128)(2,1)} %value_ref.1, bf16[64,4096]{1,0:T(8,128)(2,1)} %bitcast.2, ...), custom_call_target="tpu_custom_call" | custom-call | tf_op jit(solution)/shard_map/pallas_call | solution.py:630
  40.0 1.5 %copy.15 = bf16[2,4,128,32]{2,3,1,0:T(8,128)(2,1)} copy(bf16[2,4,128,32]{2,3,1,0:T(8,128)(2,1)} %bitcast.3) | data formatting | bytes 131072
  41.4 1.2 %copy.16 = bf16[2,4,32]{2,1,0:T(4,128)(2,1)} copy(bf16[2,4,32]{2,1,0:T(4,128)(2,1)} %get-tuple-element.9) | data formatting | bytes 1024
where the time goes:
time: 42.9 us; the launch traced here: 42.7 us
  Pallas kernels  39.3 us (92%)
  local copies, waits for them, and re-layouts  2.72 us (6%)
  between operations  0.64 us (1%)
    pallas_call x1, Pallas kernels, local_fused(): pl.pallas_call(functools.partial(fused_kernel, sp_size, tp_size), out_sha...  39.3 us
    unnamed x2, local copies, waits for them, and re-layouts  2.72 us

commit v1 on v0

--- a/solution.py
+++ b/solution.py
@@ -600,6 +600,17 @@
                         piece(origin, s, other, onward * CORES + core).wait_send()
 
 
+def place_kernel(state_ref, read_ref, state_hbm, read_hbm, sem):
+    copies = [
+        pltpu.make_async_copy(state_ref, state_hbm, sem.at[0]),
+        pltpu.make_async_copy(read_ref, read_hbm, sem.at[1]),
+    ]
+    for copy in copies:
+        copy.start()
+    for copy in copies:
+        copy.wait()
+
+
 def local_fused(
     tokens,
     key_matrix,
@@ -630,8 +641,8 @@
     turned, read = pl.pallas_call(
         functools.partial(fused_kernel, sp_size, tp_size),
         out_shape=(
-            jax.ShapeDtypeStruct((sequences, local_heads, share, key_width), jnp.bfloat16),
-            jax.ShapeDtypeStruct((sequences, local_heads, share), jnp.bfloat16),
+            pltpu.VMEM((sequences, local_heads, share, key_width), jnp.bfloat16),
+            pltpu.VMEM((sequences, local_heads, share), jnp.bfloat16),
         ),
         in_specs=[smem, smem] + [anywhere] * 9,
         out_specs=(vmem, vmem),
@@ -683,6 +694,13 @@
         next_token_value,
         read_norm_gain,
     )
+    turned, read = pl.pallas_call(
+        place_kernel,
+        out_shape=tuple(jax.ShapeDtypeStruct(a.shape, a.dtype) for a in (turned, read)),
+        in_specs=[vmem, vmem],
+        out_specs=(anywhere, anywhere),
+        scratch_shapes=[dma((2,))],
+    )(*(pltpu.with_memory_space_constraint(a, pltpu.VMEM) for a in (turned, read)))
     return jnp.swapaxes(turned, 2, 3), read
 
 

time: 42.9 us -> 40.2 us (0.937)
  local copies, waits for them, and re-layouts: 2.72 us -> 0 us
    unnamed x2 -> x0, local copies, waits for them, and re-layouts: 2.72 us -> none
    pallas_call x0 -> x1, Pallas kernels: none -> 0.65 us  [local_fused(): pl.pallas_call(place_kernel, out_shape=tuple((jax.ShapeDtypeStruct(a.shap...]
    pallas_call x1, Pallas kernels: 39.3 us -> 38.7 us  [local_fused(): pl.pallas_call(functools.partial(fused_kernel, sp_size, tp_size), out_sha...]
where the time goes in v1:
time: 40.2 us; the launch traced here: 40 us
  Pallas kernels  39.4 us (98%)
  between operations  0.64 us (2%)
    pallas_call x1, Pallas kernels, local_fused(): pl.pallas_call(functools.partial(fused_kernel, sp_size, tp_size), out_sha...  38.7 us

profile of v1, /device:TPU:0, one launch (start us, length us, event | category | flops | bytes accessed | tf_op | source)
XLA Modules:
  0.0 40.0 jit_solution(9963905297760125102)
XLA Ops:
  0.6 38.7 %shard_map.122 = (bf16[2,4,32,128]{3,2,1,0:T(8,128)(2,1)S(1)}, bf16[2,4,32]{2,1,0:T(4,128)(2,1)S(1)}) custom-call(f32[4]{0:T(128)} %rate_ref.1, f32[2,4]{1,0:T(2,128)} %next_strength_ref.1, bf16[2,128,512]{2,1,0:T(8,128)(2,1)} %tokens_ref.1, bf16[4096,512]{1,0:T(8,128)(2,1)} %key_ref.1, bf16[4096,512]{1,0:T(8,128)(2,1)} %value_ref.1, ...), custom_call_target="tpu_custom_call" | custom-call | tf_op jit(solution)/shard_map/pallas_call | solution.py:641
  39.3 0.7 %shard_map.123 = (bf16[2,4,32,128]{3,2,1,0:T(8,128)(2,1)}, bf16[2,4,32]{2,1,0:T(4,128)(2,1)}) custom-call(bf16[2,4,32,128]{3,2,1,0:T(8,128)(2,1)S(1)} %get-tuple-element.6.state_ref, bf16[2,4,32]{2,1,0:T(4,128)(2,1)S(1)} %get-tuple-element.7.read_ref), custom_call_target="tpu_custom_call" | custom-call | tf_op jit(solution)/shard_map/pallas_call | solution.py:697

commit v2 on v1

v2 whole, which is shorter than its diff:
```python
import functools

import jax
import jax.numpy as jnp
from jax import lax
from jax.experimental import pallas as pl
from jax.experimental.pallas import tpu as pltpu
from jax.sharding import PartitionSpec as P

DV = 128
CORES = 2
MESH = pl.DeviceIdType.MESH


exact_mode = lax.Precision.HIGHEST
strength_offset = 5.0


def unit_rows(matrix):
    return matrix * lax.rsqrt(jnp.sum(matrix * matrix, axis=-1, keepdims=True) + 1e-06)


def nilpotent_inverse(mixing):
    extent = mixing.shape[-1]
    result = jnp.zeros_like(mixing) + jnp.eye(extent, dtype=jnp.float32)
    powered = -mixing
    covered = 1
    while covered < extent:
        product = lax.optimization_barrier(
            jnp.einsum("...ij,...jk->...ik", result, powered, precision=exact_mode)
        )
        result = result + product
        powered = jnp.einsum("...ij,...jk->...ik", powered, powered, precision=exact_mode)
        covered = covered * 2
    return result


def block_terms(unit_keys, values, decay_logarithm, strength):
    extent = unit_keys.shape[-2]
    lower = jnp.tril(jnp.ones((extent, extent), jnp.bool_))
    strict = jnp.tril(jnp.ones((extent, extent), jnp.bool_), -1)
    running = jnp.cumsum(decay_logarithm, axis=-1)
    spread = running[..., :, None] - running[..., None, :]
    within = jnp.where(lower, jnp.exp(jnp.where(lower, spread, 0.0)), 0.0)
    scaled = unit_keys * strength[..., None]
    mixing = jnp.where(
        strict,
        jnp.einsum("...id,...jd->...ij", scaled, unit_keys, precision=exact_mode) * within,
        0.0,
    )
    inverse = nilpotent_inverse(mixing)
    writes = jnp.einsum(
        "...ij,...je->...ie", inverse, values * strength[..., None], precision=exact_mode
    )
    erases = jnp.einsum(
        "...ij,...jd->...id", inverse, scaled * jnp.exp(running)[..., None], precision=exact_mode
    )
    final_log = running[..., -1]
    carried = unit_keys * jnp.exp(final_log[..., None] - running)[..., None]
    return (writes, erases, carried, final_log)


def split_blocks(array, block_count):
    shaped = array.reshape(
        array.shape[:2] + (block_count, array.shape[2] // block_count) + array.shape[3:]
    )
    return jnp.moveaxis(shaped, 2, 0)


def local_general(
    tokens,
    key_matrix,
    value_matrix,
    gate_matrix,
    head_decay_rate,
    extra_log_decay,
    next_token_query,
    next_token_key,
    next_token_value,
    next_write_strength,
    read_norm_gain,
):
    sequences, positions, _ = tokens.shape
    local_heads = head_decay_rate.shape[0]
    key_width = key_matrix.shape[1] // local_heads
    value_width = value_matrix.shape[1] // local_heads
    all_heads = gate_matrix.shape[1] // 2
    group_size = lax.axis_size("sp")
    column_share = value_width // group_size
    first_head = lax.axis_index("tp") * local_heads
    decay_cols = lax.dynamic_slice_in_dim(gate_matrix, first_head, local_heads, 1)
    strength_cols = lax.dynamic_slice_in_dim(gate_matrix, all_heads + first_head, local_heads, 1)
    gate_cols = jnp.concatenate([decay_cols, strength_cols], axis=1)
    row_count = sequences * positions
    incoming = lax.all_gather(tokens, "tp", axis=2, tiled=True)
    span_width = incoming.shape[2]
    flat_rows = incoming.reshape(row_count, span_width)
    products = lax.optimization_barrier(
        (
            jnp.dot(flat_rows, key_matrix, preferred_element_type=jnp.float32),
            jnp.dot(flat_rows, value_matrix, preferred_element_type=jnp.float32),
            jnp.dot(flat_rows, gate_cols, preferred_element_type=jnp.float32),
        )
    )
    key_sum = products[0]
    value_sum = products[1]
    gate_pre = products[2]
    key_float = lax.optimization_barrier(key_sum.astype(jnp.bfloat16)).astype(jnp.float32)
    value_float = lax.optimization_barrier(value_sum.astype(jnp.bfloat16)).astype(jnp.float32)
    unit_keys = unit_rows(
        key_float.reshape(sequences, positions, local_heads, key_width).transpose(0, 2, 1, 3)
    )
    values = value_float.reshape(sequences, positions, local_heads, value_width).transpose(
        0, 2, 1, 3
    )
    gate_projected = gate_pre.reshape(sequences, positions, 2 * local_heads).transpose(0, 2, 1)
    decay_logarithm = (
        -head_decay_rate[None, :, None] * jax.nn.softplus(gate_projected[:, :local_heads])
        + extra_log_decay
    )
    strength = jax.nn.sigmoid(gate_projected[:, local_heads:] - strength_offset)
    block_count = positions // min(64, positions)
    block_parts = block_terms(
        split_blocks(unit_keys, block_count),
        split_blocks(values, block_count),
        split_blocks(decay_logarithm, block_count),
        split_blocks(strength, block_count),
    )
    identity = jnp.zeros((sequences, local_heads, key_width, key_width), jnp.float32) + jnp.eye(
        key_width, dtype=jnp.float32
    )
    start_map = jnp.concatenate(
        [identity, jnp.zeros((sequences, local_heads, key_width, value_width), jnp.float32)],
        axis=-1,
    )

    def advance(current, block_part):
        writes, erases, carried, final_log = block_part
        padded = jnp.concatenate(
            [jnp.zeros(writes.shape[:-1] + (key_width,), jnp.float32), writes], axis=-1
        )
        removed = lax.optimization_barrier(
            jnp.einsum("shcd,shde->shce", erases, current, precision=exact_mode)
        )
        fresh = padded - removed
        added = lax.optimization_barrier(
            jnp.einsum("shcd,shce->shde", carried, fresh, precision=exact_mode)
        )
        current = current * jnp.exp(final_log)[..., None, None] + added
        return (current, None)

    local_map, _ = lax.scan(advance, start_map, block_parts)
    carry_map = local_map[..., :key_width]
    write_map = local_map[..., key_width:]
    carry_copies = jnp.broadcast_to(carry_map[None], (group_size,) + carry_map.shape)
    write_parts = jnp.moveaxis(
        write_map.reshape(sequences, local_heads, key_width, group_size, column_share), 3, 0
    )
    carries = lax.all_to_all(carry_copies, "sp", split_axis=0, concat_axis=0, tiled=True)
    write_cols = lax.all_to_all(write_parts, "sp", split_axis=0, concat_axis=0, tiled=True)

    def fold_step(current, block_map):
        moved = lax.optimization_barrier(
            jnp.einsum("shij,shje->shie", block_map[0], current, precision=exact_mode)
        )
        return (moved + block_map[1], None)

    begin_state = jnp.zeros(write_cols.shape[1:], jnp.float32)
    folded, _ = lax.scan(fold_step, begin_state, (carries, write_cols))
    query_rows = next_token_query.astype(jnp.float32).reshape(sequences, local_heads, key_width)
    unit_new = unit_rows(
        next_token_key.astype(jnp.float32).reshape(sequences, local_heads, key_width)
    )
    value_rows = next_token_value.astype(jnp.float32)
    key_read = jnp.einsum("shd,shde->she", unit_new, folded, precision=exact_mode)
    query_read = jnp.einsum("shd,shde->she", query_rows, folded, precision=exact_mode)
    intersection = jnp.sum(query_rows * unit_new, axis=-1)
    read_raw = query_read + (next_write_strength * intersection)[..., None] * (
        value_rows - key_read
    )
    square_total = lax.psum(jnp.sum(read_raw * read_raw, axis=-1, keepdims=True), "sp")
    first_read = read_raw * lax.rsqrt(square_total / DV + 1e-06) * read_norm_gain
    return (folded.astype(jnp.bfloat16), first_read.astype(jnp.bfloat16))


def short_dot(left, right, contract=((1,), (0,))):
    return lax.dot_general(
        left.astype(jnp.bfloat16),
        right.astype(jnp.bfloat16),
        (contract, ((), ())),
        preferred_element_type=jnp.float32,
    )


def three_terms(x):
    first = x.astype(jnp.bfloat16)
    rest = x - first.astype(jnp.float32)
    second = rest.astype(jnp.bfloat16)
    third = (rest - second.astype(jnp.float32)).astype(jnp.bfloat16)
    return first, second, third


def softplus(x):
    return jnp.maximum(x, 0.0) + jnp.log1p(jnp.exp(-jnp.abs(x)))


def grid_mask(rows, cols, rule):
    row = lax.broadcasted_iota(jnp.int32, (rows, cols), 0)
    col = lax.broadcasted_iota(jnp.int32, (rows, cols), 1)
    return rule(row, col)


def compose(late, early):
    late_map, late_write, late_keep = late
    early_map, early_write, early_keep = early
    width = early_map.shape[1]
    moved = short_dot(late_map, jnp.concatenate([early_map, early_write], axis=1))
    return (
        late_keep * early_map + early_keep * late_map - moved[:, :width],
        late_keep * early_write + late_write - moved[:, width:],
        late_keep * early_keep,
    )


def compose_write(late, early_write):
    late_map, late_write, late_keep = late
    return late_keep * early_write + late_write - short_dot(late_map, early_write)


def fused_kernel(
    sp_size,
    tp_size,
    rate_ref,
    next_strength_ref,
    tokens_ref,
    key_ref,
    value_ref,
    gate_hbm,
    extra_hbm,
    query_hbm,
    new_key_hbm,
    new_value_hbm,
    gain_hbm,
    state_ref,
    read_ref,
    gathered,
    key_w,
    value_w,
    gate_ref,
    gate_own,
    extra_ref,
    query_ref,
    new_key_ref,
    new_value_ref,
    gain_ref,
    key_acc,
    value_acc,
    gate_acc,
    key_out,
    key_in,
    value_out,
    value_in,
    side_out,
    side_in,
    state_out,
    row_out,
    row_in,
    load_sem,
    weight_sem,
    gather_recv,
    gather_send,
    swap_recv,
    swap_send,
    last_recv,
    last_send,
    above_sem,
    peers_sem,
):
    sequences, positions, depth = tokens_ref.shape
    local_heads = extra_ref.shape[1]
    key_width = key_acc.shape[1] // local_heads
    value_width = value_acc.shape[1] // local_heads
    share = value_width // sp_size
    all_heads = gate_ref.shape[0] // 2
    chips = tp_size // CORES
    me = lax.axis_index("sp")
    spot = lax.axis_index("tp")
    chip = spot // CORES
    core = spot % CORES
    partner = chip * CORES + (1 - core)
    half = positions // 2
    units = [(s, part * half, half) for s in range(sequences) for part in range(2)]
    last_unit = len(units) - 1
    batches = [(0, 0, positions, (0, 1)), (1, 0, half, (2,)), (1, half, half, (3,))]
    others = [sp_size - 1 - me, me + 1 - 2 * (me % 2), (me + 2) % sp_size]

    loads = [
        pltpu.make_async_copy(tokens_ref.at[s], gathered.at[spot, s], load_sem.at[s])
        for s in range(sequences)
    ]
    for load in loads:
        load.start()

    barrier = pltpu.get_barrier_semaphore()
    pl.semaphore_signal(barrier, inc=1, device_id={"tp": partner}, device_id_type=MESH)

    @pl.when(chip < chips - 1)
    def _():
        pl.semaphore_signal(barrier, inc=1, device_id={"tp": spot + CORES}, device_id_type=MESH)

    for other in range(1, sp_size):

        @pl.when(me < other)
        def _(other=other):
            pl.semaphore_signal(barrier, inc=1, device_id={"sp": other}, device_id_type=MESH)

    weights = [
        pltpu.make_async_copy(key_ref, key_w, weight_sem.at[0]),
        pltpu.make_async_copy(value_ref, value_w, weight_sem.at[1]),
        pltpu.make_async_copy(gate_hbm, gate_ref, weight_sem.at[2]),
        pltpu.make_async_copy(extra_hbm, extra_ref, weight_sem.at[3]),
        pltpu.make_async_copy(query_hbm, query_ref, weight_sem.at[4]),
        pltpu.make_async_copy(new_key_hbm, new_key_ref, weight_sem.at[5]),
        pltpu.make_async_copy(new_value_hbm, new_value_ref, weight_sem.at[6]),
        pltpu.make_async_copy(gain_hbm, gain_ref, weight_sem.at[7]),
    ]
    for weight in weights:
        weight.start()
    pl.semaphore_wait(barrier, jnp.where(chip > 0, 1, 0) + 1 + me)

    @pl.when(chip > 0)
    def _():
        pl.semaphore_signal(above_sem, inc=1, device_id={"tp": spot - CORES}, device_id_type=MESH)

    for other in range(sp_size - 1):

        @pl.when(other < me)
        def _(other=other):
            pl.semaphore_signal(peers_sem, inc=1, device_id={"sp": other}, device_id_type=MESH)

    def piece(origin, u, way, target):
        s, low, count = units[u]
        block = gathered.at[origin, s, pl.ds(low, count)]
        return pltpu.make_async_remote_copy(
            src_ref=block,
            dst_ref=block,
            send_sem=gather_send.at[origin, u, way],
            recv_sem=gather_recv.at[origin, u],
            device_id={"tp": target},
            device_id_type=MESH,
        )

    for load in loads:
        load.wait()

    for u in range(len(units)):

        @pl.when((chip > 0) if u < last_unit else (chip == chips - 1))
        def _(u=u):
            piece(spot, u, 1, spot - CORES).start()

        piece(spot, u, 2, partner).start()

    @pl.when(chip < chips - 1)
    def _():
        pl.semaphore_wait(above_sem, 1)

    for u in range(len(units)):

        @pl.when((chip < chips - 1) if u < last_unit else (chip == 0))
        def _(u=u):
            piece(spot, u, 0, spot + CORES).start()

    key_acc[...] = jnp.zeros_like(key_acc)
    value_acc[...] = jnp.zeros_like(value_acc)
    gate_acc[...] = jnp.zeros_like(gate_acc)
    side_out[...] = jnp.zeros_like(side_out)

    def add_in(rows, span, batch):
        s, low, count, parts = batches[batch]
        cut = slice(s * positions + low, s * positions + low + count)
        key_acc[cut] += jnp.dot(rows, key_w[span, :], preferred_element_type=jnp.float32)
        value_acc[cut] += jnp.dot(rows, value_w[span, :], preferred_element_type=jnp.float32)
        gates = lax.dot_general(
            gate_own[:, span],
            rows,
            (((1,), (1,)), ((), ())),
            preferred_element_type=jnp.float32,
        )
        gate_acc[s, :, low : low + count] += gates

    def take_one(block, batch):
        s, low, count, _ = batches[batch]
        span = pl.ds(pl.multiple_of(block * depth, depth), depth)
        add_in(gathered[block, s, low : low + count], span, batch)

    def take_chip(origin_chip, batch):
        s, low, count, _ = batches[batch]
        width = CORES * depth
        span = pl.ds(pl.multiple_of(origin_chip * width, width), width)
        rows = jnp.concatenate(
            [gathered[origin_chip * CORES + c, s, low : low + count] for c in range(CORES)], axis=1
        )
        add_in(rows, span, batch)

    first = spot * local_heads

    def prepare():
        for weight in weights:
            weight.wait()
        chooser = grid_mask(
            2 * local_heads,
            2 * all_heads,
            lambda r, c: c
            == jnp.where(r < local_heads, first + r, all_heads + first + r - local_heads),
        ).astype(jnp.float32)
        gate_own[...] = short_dot(chooser, gate_ref[...]).astype(jnp.bfloat16)
        placer = grid_mask(share, value_width, lambda r, c: c == me * share + r)
        for s in range(sequences):
            new_value = short_dot(new_value_ref[s], placer.astype(jnp.float32))
            for h in range(local_heads):
                side_out[h, s, 2:3, :] = new_value[h : h + 1, :]

    def own(batch):
        for u in batches[batch][3]:
            piece(partner, u, 2, partner).wait_recv()
        take_chip(chip, batch)

    def relay(distance, u):
        for way, step in ((0, -1), (1, 1)):
            origin_chip = chip + step * distance
            origin = origin_chip * CORES + core
            present = (origin_chip >= 0) & (origin_chip < chips)
            onward = chip - step
            beyond = (onward >= 0) & (onward < chips)

            @pl.when(present)
            def _(way=way, origin_chip=origin_chip, origin=origin, onward=onward, beyond=beyond):
                piece(origin, u, way, partner).wait_recv()

                @pl.when(beyond)
                def _():
                    piece(origin, u, way, onward * CORES + core).start()

                piece(origin, u, 2, partner).start()
                if u == 1:

                    @pl.when(beyond & (origin_chip == (0 if way == 0 else chips - 1)))
                    def _():
                        piece(spot, last_unit, way, onward * CORES + core).start()

    def absorb(distance, batch):
        def one_side(side, carry):
            origin_chip = chip + (2 * side - 1) * distance

            @pl.when((origin_chip >= 0) & (origin_chip < chips))
            def _():
                for u in batches[batch][3]:
                    piece(origin_chip * CORES + 1 - core, u, 2, partner).wait_recv()
                take_chip(origin_chip, batch)

            return carry

        lax.fori_loop(0, 2, one_side, 0)

    def absorb_lane(distance, batch, lane):
        def one_side(side, carry):
            origin_chip = chip + (2 * side - 1) * distance

            @pl.when((origin_chip >= 0) & (origin_chip < chips))
            def _():
                block = origin_chip * CORES + (core if lane == 0 else 1 - core)
                if lane:
                    for u in batches[batch][3]:
                        piece(block, u, 2, partner).wait_recv()
                take_one(block, batch)

            return carry

        lax.fori_loop(0, 2, one_side, 0)

    def swap(n, slot, target, origin):
        s, low, count, _ = batches[slot]
        if n == 0:
            source, sink = side_out.at[target, slot], side_in.at[origin, slot]
        else:
            source, sink = ((key_out, key_in), (value_out, value_in))[n - 1]
            source = source.at[target, s, pl.ds(low, count)]
            sink = sink.at[origin, s, pl.ds(low, count)]
        return pltpu.make_async_remote_copy(
            src_ref=source,
            dst_ref=sink,
            send_sem=swap_send.at[n, slot, target],
            recv_sem=swap_recv.at[n, slot, origin],
            device_id={"sp": target},
            device_id_type=MESH,
        )

    def hand_out(slot):
        s, low, count, _ = batches[slot]
        cut = slice(s * positions + low, s * positions + low + count)
        gates = gate_acc[s, :, low : low + count]
        extra = extra_ref[s, :, low : low + count]
        for h in range(local_heads):
            side_out[h, slot, 0:1, low : low + count] = (
                -rate_ref[h] * softplus(gates[h : h + 1]) + extra[h : h + 1, :]
            )
            side_out[h, slot, 1:2, low : low + count] = jax.nn.sigmoid(
                gates[local_heads + h : local_heads + h + 1] - strength_offset
            )
        for other in others:
            swap(0, slot, other, me).start()
        for h in range(local_heads):
            key_out[h, s, low : low + count] = key_acc[
                cut, h * key_width : (h + 1) * key_width
            ].astype(jnp.bfloat16)
        for other in others:
            swap(1, slot, other, me).start()
        for h in range(local_heads):
            value_out[h, s, low : low + count] = value_acc[
                cut, h * value_width : (h + 1) * value_width
            ].astype(jnp.bfloat16)
        for other in others:
            swap(2, slot, other, me).start()
        side_in[me, slot] = side_out[me, slot]
        key_in[me, s, low : low + count] = key_out[me, s, low : low + count]
        value_in[me, s, low : low + count] = value_out[me, s, low : low + count]

    far = chips - 1
    last_batch = len(batches) - 1
    steps = {1: [(1, 0), (1, 1), (1, 2)]} if far > 1 else {}
    for distance in range(2, far):
        steps[distance] = [(distance, 0), (distance, 1), (distance, 2)]
    work = [(own, (0,)), (own, (1,)), (own, (2,))]
    prepared = False
    for distance in range(1, far):
        for event in steps[distance]:
            relay(*event)
            if not prepared:
                prepare()
                prepared = True
            if work:
                act, operands = work.pop(0)
                act(*operands)
            if event[1] == 1:
                work.insert(0, (absorb, (distance, 0)))
            if event[1] == 2:
                work.append((absorb, (distance, 1)))
    if not prepared:
        prepare()
    for act, operands in [w for w in work if w[0] is own]:
        act(*operands)
    work = [w for w in work if w[0] is absorb]
    relay(far, 0)
    for act, operands in [w for w in work if w[1][1] == 0]:
        act(*operands)
    work = [w for w in work if w[1][1] != 0]
    relay(far, 1)
    absorb(far, 0)

    @pl.when(me < sp_size - 1)
    def _():
        pl.semaphore_wait(peers_sem, sp_size - 1 - me)

    hand_out(0)
    if far > 1:
        relay(1, last_unit)
    for act, operands in work:
        act(*operands)
    relay(far, 2)
    if far > 1:
        absorb(1, last_batch)
    absorb(far, 1)
    hand_out(1)
    pending = None
    for distance in range(2, far):
        relay(distance, last_unit)
        if pending is not None:
            absorb(*pending)
        pending = (distance, last_batch)
    relay(far, last_unit)
    if pending is not None:
        absorb(*pending)
    absorb_lane(far, last_batch, 0)
    absorb_lane(far, last_batch, 1)
    hand_out(2)

    for u in range(len(units)):
        piece(spot, u, 2, partner).wait_send()

        @pl.when(chip < chips - 1)
        def _(u=u):
            piece(spot, u, 0, spot + CORES).wait_send()

        @pl.when(chip > 0)
        def _(u=u):
            piece(spot, u, 1, spot - CORES).wait_send()

        for distance in range(1, chips):
            for way, step in ((0, -1), (1, 1)):
                origin_chip = chip + step * distance
                origin = origin_chip * CORES + core
                onward = chip - step
                present = (origin_chip >= 0) & (origin_chip < chips)

                @pl.when(present)
                def _(u=u, origin=origin):
                    piece(origin, u, 2, partner).wait_send()

                @pl.when(present & (onward >= 0) & (onward < chips))
                def _(u=u, origin=origin, way=way, onward=onward):
                    piece(origin, u, way, onward * CORES + core).wait_send()

    side_rows = side_in.shape[2]
    upto = grid_mask(positions, positions, lambda r, c: r <= c).astype(jnp.float32)
    down = jnp.concatenate(
        [
            grid_mask(positions, positions, lambda r, c: c <= r).astype(jnp.float32),
            grid_mask(positions, positions, lambda r, c: c == r).astype(jnp.float32),
        ],
        axis=0,
    )
    lanes = pl.ds(pl.multiple_of(me * key_width, key_width), key_width)
    queries = query_ref[:, lanes].astype(jnp.float32)
    new_keys = new_key_ref[:, lanes].astype(jnp.float32)
    new_keys = new_keys * lax.rsqrt(jnp.sum(new_keys * new_keys, axis=-1, keepdims=True) + 1e-06)
    meets = jnp.sum(queries * new_keys, axis=-1, keepdims=True)

    def block_maps(s, slots):
        count = positions
        eye = grid_mask(count, count, lambda r, c: r == c).astype(jnp.float32)
        lower = grid_mask(count, count, lambda r, c: r >= c)
        strict = grid_mask(count, count, lambda r, c: r > c)
        for slot in slots:
            for other in others:
                swap(0, slot, other, other).wait_recv()
        side = three_terms(
            sum(side_in[:, slot].reshape(sp_size * side_rows, positions) for slot in slots)
        )
        running_row = sum(short_dot(term, upto) for term in side)
        columns = sum(short_dot(down, term, ((1,), (1,))) for term in side)
        for slot in slots:
            for other in others:
                swap(1, slot, other, other).wait_recv()
        parts = []
        for b in range(sp_size):
            line = b * side_rows
            row = running_row[line : line + 1, :]
            col = columns[:positions, line : line + 1]
            strength = columns[positions:, line + 1 : line + 2]
            final_log = row[:, count - 1 : count]
            keys = key_in[b, s].astype(jnp.float32)
            keys = keys * lax.rsqrt(jnp.sum(keys * keys, axis=-1, keepdims=True) + 1e-06)
            within = jnp.where(lower, jnp.exp(jnp.where(lower, col - row, 0.0)), 0.0)
            scaled = keys * strength
            power = jnp.where(strict, -short_dot(scaled, keys, ((1,), (1,))) * within, 0.0)
            erased = scaled * jnp.exp(col)
            carried = (keys * jnp.exp(final_log - col)).T.astype(jnp.bfloat16)
            parts.append([eye + power, power, strength, erased, carried, jnp.exp(final_log)])
        for part in parts:
            part[1] = short_dot(part[1], part[1])
        covered = 2
        while covered < count:
            for part in parts:
                if covered * 2 < count:
                    both = short_dot(part[1], jnp.concatenate([part[0], part[1]], axis=1))
                    part[0] = part[0] + both[:, :count]
                    part[1] = both[:, count:]
                else:
                    part[0] = part[0] + short_dot(part[1], part[0])
            covered = covered * 2
        for slot in slots:
            for other in others:
                swap(2, slot, other, other).wait_recv()
        solved = []
        for b, part in enumerate(parts):
            values = value_in[b, s].astype(jnp.float32) * part[2]
            solved.append(short_dot(part[0], jnp.concatenate([part[3], values], axis=1)))
        maps = []
        for part, both in zip(parts, solved):
            both = short_dot(part[4], both)
            maps.append((both[:, :key_width], both[:, key_width:], part[5]))
        return maps

    def final(n, s, target, origin):
        source, sink = (
            (state_out.at[target, s], state_ref.at[s, origin]),
            (row_out.at[target, s], row_in.at[origin, s]),
        )[n]
        return pltpu.make_async_remote_copy(
            src_ref=source,
            dst_ref=sink,
            send_sem=last_send.at[n, s, target],
            recv_sem=last_recv.at[n, s, origin],
            device_id={"sp": target},
            device_id_type=MESH,
        )

    def finish(s, maps):
        while len(maps) > 2:
            maps = [compose(maps[i + 1], maps[i]) for i in range(0, len(maps), 2)]
        state = compose_write(maps[1], maps[0][1])
        wide = (8, key_width)
        first_row = grid_mask(*wide, lambda r, c: r == 0)
        probes = jnp.where(
            first_row,
            jnp.broadcast_to(queries[s : s + 1], wide),
            jnp.broadcast_to(new_keys[s : s + 1], wide),
        )
        probe_terms, state_terms = three_terms(probes)[:2], three_terms(state)[:2]
        reads = (
            short_dot(probe_terms[0], state_terms[0])
            + short_dot(probe_terms[0], state_terms[1])
            + short_dot(probe_terms[1], state_terms[0])
        )
        turned = state.T.astype(jnp.bfloat16)
        for j in range(sp_size):
            state_out[j, s] = turned[j * share : (j + 1) * share, :]
        for other in others:
            final(0, s, other, me).start()
        query_read, key_read = reads[0:1], reads[1:2]
        new_value = jnp.sum(side_in[:, s, 2, :], axis=0, keepdims=True)
        raw = query_read + (next_strength_ref[s, me] * meets[s : s + 1]) * (new_value - key_read)
        raw = raw * lax.rsqrt(jnp.sum(raw * raw, axis=-1, keepdims=True) / value_width + 1e-06)
        for j in range(sp_size):
            turn = j * share
            row_out[j, s, 0:1, :] = (
                jnp.concatenate([raw[:, turn:], raw[:, :turn]], axis=1) if j else raw
            )
        for other in others:
            final(1, s, other, me).start()
        state_ref[s, me] = state_out[me, s]
        row_in[me, s] = row_out[me, s]

    row_out[...] = jnp.zeros_like(row_out)
    finish(0, block_maps(0, (0,)))
    finish(1, block_maps(1, (1, 2)))

    for slot in range(len(batches)):
        for n in range(3):
            for other in others:
                swap(n, slot, other, me).wait_send()
    for s in range(sequences):
        for n in range(2):
            for other in others:
                final(n, s, other, me).wait_send()
    for s in range(sequences):
        for other in others:
            final(1, s, other, other).wait_recv()
        rows = jnp.concatenate([row_in[i, s, 0:1, :share] for i in range(sp_size)], axis=0)
        read_ref[s] = (rows * gain_ref[...].reshape(1, share)).astype(jnp.bfloat16)
    for s in range(sequences):
        for other in others:
            final(0, s, other, other).wait_recv()


def place_kernel(state_ref, read_ref, state_hbm, read_hbm, sem):
    copies = [
        pltpu.make_async_copy(state_ref, state_hbm, sem.at[0]),
        pltpu.make_async_copy(read_ref, read_hbm, sem.at[1]),
    ]
    for copy in copies:
        copy.start()
    for copy in copies:
        copy.wait()


def local_fused(
    tokens,
    key_matrix,
    value_matrix,
    gate_matrix,
    head_decay_rate,
    extra_log_decay,
    next_token_query,
    next_token_key,
    next_token_value,
    next_write_strength,
    read_norm_gain,
):
    sequences, positions, depth = tokens.shape
    local_heads = head_decay_rate.shape[0]
    sp_size = lax.axis_size("sp")
    tp_size = lax.axis_size("tp")
    key_total = key_matrix.shape[1]
    value_total = value_matrix.shape[1]
    key_width = key_total // local_heads
    value_width = value_total // local_heads
    share = value_width // sp_size
    rows = sequences * positions
    units = 2 * sequences
    slots = sequences + 1
    vmem = pl.BlockSpec(memory_space=pltpu.VMEM)
    smem = pl.BlockSpec(memory_space=pltpu.SMEM)
    anywhere = pl.BlockSpec(memory_space=pl.ANY)
    dma = pltpu.SemaphoreType.DMA
    held = (sp_size, sequences, positions)
    turned, read = pl.pallas_call(
        functools.partial(fused_kernel, sp_size, tp_size),
        out_shape=(
            pltpu.VMEM((sequences, local_heads, share, key_width), jnp.bfloat16),
            pltpu.VMEM((sequences, local_heads, share), jnp.bfloat16),
        ),
        in_specs=[smem, smem] + [anywhere] * 9,
        out_specs=(vmem, vmem),
        scratch_shapes=[
            pltpu.VMEM((tp_size, sequences, positions, depth), jnp.bfloat16),
            pltpu.VMEM(key_matrix.shape, jnp.bfloat16),
            pltpu.VMEM(value_matrix.shape, jnp.bfloat16),
            pltpu.VMEM(gate_matrix.shape[::-1], jnp.bfloat16),
            pltpu.VMEM((2 * local_heads, gate_matrix.shape[0]), jnp.bfloat16),
            pltpu.VMEM(extra_log_decay.shape, jnp.float32),
            pltpu.VMEM(next_token_query.shape, jnp.bfloat16),
            pltpu.VMEM(next_token_key.shape, jnp.bfloat16),
            pltpu.VMEM(next_token_value.shape, jnp.bfloat16),
            pltpu.VMEM(read_norm_gain.shape, jnp.float32),
            pltpu.VMEM((rows, key_total), jnp.float32),
            pltpu.VMEM((rows, value_total), jnp.float32),
            pltpu.VMEM((sequences, 2 * local_heads, positions), jnp.float32),
            pltpu.VMEM((*held, key_width), jnp.bfloat16),
            pltpu.VMEM((*held, key_width), jnp.bfloat16),
            pltpu.VMEM((*held, value_width), jnp.bfloat16),
            pltpu.VMEM((*held, value_width), jnp.bfloat16),
            pltpu.VMEM((sp_size, slots, 8, positions), jnp.float32),
            pltpu.VMEM((sp_size, slots, 8, positions), jnp.float32),
            pltpu.VMEM((sp_size, sequences, share, key_width), jnp.bfloat16),
            pltpu.VMEM((sp_size, sequences, 8, value_width), jnp.float32),
            pltpu.VMEM((sp_size, sequences, 8, value_width), jnp.float32),
            dma((sequences,)),
            dma((8,)),
            dma((tp_size, units)),
            dma((tp_size, units, 3)),
            dma((3, slots, sp_size)),
            dma((3, slots, sp_size)),
            dma((2, sequences, sp_size)),
            dma((2, sequences, sp_size)),
            pltpu.SemaphoreType.REGULAR,
            pltpu.SemaphoreType.REGULAR,
        ],
        compiler_params=pltpu.CompilerParams(
            collective_id=0, has_side_effects=True
        ),
    )(
        head_decay_rate,
        next_write_strength,
        tokens,
        key_matrix,
        value_matrix,
        gate_matrix.T,
        extra_log_decay,
        next_token_query,
        next_token_key,
        next_token_value,
        read_norm_gain,
    )
    turned, read = pl.pallas_call(
        place_kernel,
        out_shape=tuple(jax.ShapeDtypeStruct(a.shape, a.dtype) for a in (turned, read)),
        in_specs=[vmem, vmem],
        out_specs=(anywhere, anywhere),
        scratch_shapes=[dma((2,))],
    )(*(pltpu.with_memory_space_constraint(a, pltpu.VMEM) for a in (turned, read)))
    return jnp.swapaxes(turned, 2, 3), read


def local(*arguments):
    tokens, key_matrix, value_matrix = arguments[:3]
    sequences, positions, _ = tokens.shape
    local_heads = arguments[4].shape[0]
    sp_size = lax.axis_size("sp")
    fits = (
        local_heads == sp_size
        and sp_size == 4
        and sequences == 2
        and 2 * local_heads == 8
        and lax.axis_size("tp") % CORES == 0
        and lax.axis_size("tp") > CORES
        and positions == key_matrix.shape[1] // local_heads
        and positions == value_matrix.shape[1] // local_heads
        and positions % 128 == 0
    )
    return local_fused(*arguments) if fits else local_general(*arguments)


def solution(mesh):
    in_specs = (
        P(None, "sp", "tp"),
        P(None, "tp"),
        P(None, "tp"),
        P(),
        P("tp"),
        P(None, "tp", "sp"),
        P(None, "tp"),
        P(None, "tp"),
        P(None, "tp", "sp"),
        P(None, "tp"),
        P("sp"),
    )
    out_specs = (P(None, "tp", None, "sp"), P(None, "tp", "sp"))
    return jax.shard_map(local, mesh=mesh, in_specs=in_specs, out_specs=out_specs, check_vma=False)
```

time: 40.2 us -> 38.5 us (0.958)
  Pallas kernels: 39.4 us -> 37.7 us
    pallas_call x1, Pallas kernels: 38.7 us -> 37.1 us  [local_fused(): pl.pallas_call(functools.partial(fused_kernel, sp_size, tp_size), out_sha...]
where the time goes in v2:
time: 38.5 us; the launch traced here: 38.4 us
  Pallas kernels  37.7 us (98%)
  between operations  0.64 us (2%)
    pallas_call x1, Pallas kernels, local_fused(): pl.pallas_call(functools.partial(fused_kernel, sp_size, tp_size), out_sha...  37.1 us

profile of v2, /device:TPU:0, one launch (start us, length us, event | category | flops | bytes accessed | tf_op | source)
XLA Modules:
  0.0 38.4 jit_solution(13736987526080359460)
XLA Ops:
  0.6 37.1 %shard_map.122 = (bf16[2,4,32,128]{3,2,1,0:T(8,128)(2,1)S(1)}, bf16[2,4,32]{2,1,0:T(4,128)(2,1)S(1)}) custom-call(f32[4]{0:T(128)} %rate_ref.1, f32[2,4]{1,0:T(2,128)} %next_strength_ref.1, bf16[2,128,512]{2,1,0:T(8,128)(2,1)} %tokens_ref.1, bf16[4096,512]{1,0:T(8,128)(2,1)} %key_ref.1, bf16[4096,512]{1,0:T(8,128)(2,1)} %value_ref.1, ...), custom_call_target="tpu_custom_call" | custom-call | tf_op jit(solution)/shard_map/pallas_call | solution.py:798
  37.7 0.7 %shard_map.123 = (bf16[2,4,32,128]{3,2,1,0:T(8,128)(2,1)}, bf16[2,4,32]{2,1,0:T(4,128)(2,1)}) custom-call(bf16[2,4,32,128]{3,2,1,0:T(8,128)(2,1)S(1)} %get-tuple-element.6.state_ref, bf16[2,4,32]{2,1,0:T(4,128)(2,1)S(1)} %get-tuple-element.7.read_ref), custom_call_target="tpu_custom_call" | custom-call | tf_op jit(solution)/shard_map/pallas_call | solution.py:856

commit v3 on v2

--- a/solution.py
+++ b/solution.py
@@ -230,8 +230,8 @@
 def fused_kernel(
     sp_size,
     tp_size,
-    rate_ref,
-    next_strength_ref,
+    rate_hbm,
+    next_strength_hbm,
     tokens_ref,
     key_ref,
     value_ref,
@@ -243,6 +243,8 @@
     gain_hbm,
     state_ref,
     read_ref,
+    rate_ref,
+    next_strength_ref,
     gathered,
     key_w,
     value_w,
@@ -323,6 +325,8 @@
         pltpu.make_async_copy(new_key_hbm, new_key_ref, weight_sem.at[5]),
         pltpu.make_async_copy(new_value_hbm, new_value_ref, weight_sem.at[6]),
         pltpu.make_async_copy(gain_hbm, gain_ref, weight_sem.at[7]),
+        pltpu.make_async_copy(rate_hbm, rate_ref, weight_sem.at[8]),
+        pltpu.make_async_copy(next_strength_hbm, next_strength_ref, weight_sem.at[9]),
     ]
     for weight in weights:
         weight.start()
@@ -353,23 +357,44 @@
     for load in loads:
         load.wait()
 
-    for u in range(len(units)):
-
-        @pl.when((chip > 0) if u < last_unit else (chip == chips - 1))
+    def hub(a_chip):
+        return jnp.where((a_chip == 0) | (a_chip == chips - 1), 0, 1)
+
+    for u in range(last_unit):
+
+        @pl.when(chip > 0)
         def _(u=u):
             piece(spot, u, 1, spot - CORES).start()
 
+    for u in [last_unit, *range(last_unit)]:
         piece(spot, u, 2, partner).start()
 
     @pl.when(chip < chips - 1)
     def _():
         pl.semaphore_wait(above_sem, 1)
 
-    for u in range(len(units)):
-
-        @pl.when((chip < chips - 1) if u < last_unit else (chip == 0))
+    for u in range(last_unit):
+
+        @pl.when(chip < chips - 1)
         def _(u=u):
             piece(spot, u, 0, spot + CORES).start()
+
+    def send_last(way):
+        onward = chip + (1 if way == 0 else -1)
+        for c in range(CORES):
+            piece(chip * CORES + c, last_unit, way, onward * CORES + hub(onward)).start()
+
+    @pl.when(core == 1)
+    def _():
+        piece(partner, last_unit, 2, partner).wait_recv()
+
+        @pl.when(chip == chips - 1)
+        def _():
+            send_last(1)
+
+        @pl.when(chip == 0)
+        def _():
+            send_last(0)
 
     key_acc[...] = jnp.zeros_like(key_acc)
     value_acc[...] = jnp.zeros_like(value_acc)
@@ -423,61 +448,90 @@
 
     def own(batch):
         for u in batches[batch][3]:
-            piece(partner, u, 2, partner).wait_recv()
+            if u == last_unit:
+
+                @pl.when(core == 0)
+                def _(u=u):
+                    piece(partner, u, 2, partner).wait_recv()
+
+            else:
+                piece(partner, u, 2, partner).wait_recv()
         take_chip(chip, batch)
 
     def relay(distance, u):
-        for way, step in ((0, -1), (1, 1)):
+        lanes = range(CORES) if u == last_unit else [core]
+        for lane in lanes:
+            relay_lane(distance, u, lane)
+
+    def relay_lane(distance, u, lane):
+        for way, step in ((1, 1), (0, -1)):
             origin_chip = chip + step * distance
-            origin = origin_chip * CORES + core
+            origin = origin_chip * CORES + lane
             present = (origin_chip >= 0) & (origin_chip < chips)
+            if u == last_unit:
+                present = present & (core == hub(chip))
             onward = chip - step
             beyond = (onward >= 0) & (onward < chips)
+            target = onward * CORES + (hub(onward) if u == last_unit else core)
 
             @pl.when(present)
-            def _(way=way, origin_chip=origin_chip, origin=origin, onward=onward, beyond=beyond):
+            def _(way=way, origin_chip=origin_chip, origin=origin, target=target, beyond=beyond):
                 piece(origin, u, way, partner).wait_recv()
 
                 @pl.when(beyond)
                 def _():
-                    piece(origin, u, way, onward * CORES + core).start()
+                    piece(origin, u, way, target).start()
 
                 piece(origin, u, 2, partner).start()
                 if u == 1:
 
-                    @pl.when(beyond & (origin_chip == (0 if way == 0 else chips - 1)))
+                    @pl.when(
+                        beyond & (core == 1) & (origin_chip == (0 if way == 0 else chips - 1))
+                    )
                     def _():
-                        piece(spot, last_unit, way, onward * CORES + core).start()
-
-    def absorb(distance, batch):
+                        send_last(way)
+
+    def both_sides(distance, act):
         def one_side(side, carry):
             origin_chip = chip + (2 * side - 1) * distance
 
             @pl.when((origin_chip >= 0) & (origin_chip < chips))
             def _():
-                for u in batches[batch][3]:
+                act(origin_chip)
+
+            return carry
+
+        lax.fori_loop(0, 2, one_side, 0)
+
+    def absorb(distance, batch):
+        def act(origin_chip):
+            for u in batches[batch][3]:
+                if u == last_unit:
+
+                    @pl.when(core != hub(chip))
+                    def _(u=u):
+                        for c in range(CORES):
+                            piece(origin_chip * CORES + c, u, 2, partner).wait_recv()
+
+                else:
                     piece(origin_chip * CORES + 1 - core, u, 2, partner).wait_recv()
-                take_chip(origin_chip, batch)
-
-            return carry
-
-        lax.fori_loop(0, 2, one_side, 0)
-
-    def absorb_lane(distance, batch, lane):
-        def one_side(side, carry):
-            origin_chip = chip + (2 * side - 1) * distance
-
-            @pl.when((origin_chip >= 0) & (origin_chip < chips))
+            take_chip(origin_chip, batch)
+
+        both_sides(distance, act)
+
+    def absorb_last_lane(distance, lane):
+        relay_lane(distance, last_unit, lane)
+
+        def act(origin_chip):
+            block = origin_chip * CORES + lane
+
+            @pl.when(core != hub(chip))
             def _():
-                block = origin_chip * CORES + (core if lane == 0 else 1 - core)
-                if lane:
-                    for u in batches[batch][3]:
-                        piece(block, u, 2, partner).wait_recv()
-                take_one(block, batch)
-
-            return carry
-
-        lax.fori_loop(0, 2, one_side, 0)
+                piece(block, last_unit, 2, partner).wait_recv()
+
+            take_one(block, len(batches) - 1)
+
+        both_sides(distance, act)
 
     def swap(n, slot, target, origin):
         s, low, count, _ = batches[slot]
@@ -578,38 +632,37 @@
         if pending is not None:
             absorb(*pending)
         pending = (distance, last_batch)
-    relay(far, last_unit)
     if pending is not None:
         absorb(*pending)
-    absorb_lane(far, last_batch, 0)
-    absorb_lane(far, last_batch, 1)
+    for lane in range(CORES):
+        absorb_last_lane(far, lane)
     hand_out(2)
 
-    for u in range(len(units)):
-        piece(spot, u, 2, partner).wait_send()
-
-        @pl.when(chip < chips - 1)
-        def _(u=u):
-            piece(spot, u, 0, spot + CORES).wait_send()
-
-        @pl.when(chip > 0)
-        def _(u=u):
-            piece(spot, u, 1, spot - CORES).wait_send()
-
-        for distance in range(1, chips):
+    def settle(u, lane):
+        last = u == last_unit
+        for distance in range(chips):
             for way, step in ((0, -1), (1, 1)):
                 origin_chip = chip + step * distance
-                origin = origin_chip * CORES + core
+                origin = origin_chip * CORES + lane
                 onward = chip - step
                 present = (origin_chip >= 0) & (origin_chip < chips)
-
-                @pl.when(present)
-                def _(u=u, origin=origin):
-                    piece(origin, u, 2, partner).wait_send()
-
-                @pl.when(present & (onward >= 0) & (onward < chips))
-                def _(u=u, origin=origin, way=way, onward=onward):
+                sends = present & (onward >= 0) & (onward < chips)
+
+                if distance or (way == 0 and not last):
+
+                    @pl.when(present & (core == hub(chip)) if last else present)
+                    def _(origin=origin):
+                        piece(origin, u, 2, partner).wait_send()
+
+                @pl.when(sends & (core == 1) if last else sends)
+                def _(origin=origin, way=way, onward=onward):
                     piece(origin, u, way, onward * CORES + core).wait_send()
+
+    for u in range(last_unit):
+        settle(u, core)
+    piece(spot, last_unit, 2, partner).wait_send()
+    for lane in range(CORES):
+        settle(last_unit, lane)
 
     side_rows = side_in.shape[2]
     upto = grid_mask(positions, positions, lambda r, c: r <= c).astype(jnp.float32)
@@ -634,14 +687,14 @@
         for slot in slots:
             for other in others:
                 swap(0, slot, other, other).wait_recv()
-        side = three_terms(
-            sum(side_in[:, slot].reshape(sp_size * side_rows, positions) for slot in slots)
-        )
-        running_row = sum(short_dot(term, upto) for term in side)
-        columns = sum(short_dot(down, term, ((1,), (1,))) for term in side)
         for slot in slots:
             for other in others:
                 swap(1, slot, other, other).wait_recv()
+        side = three_terms(
+            sum(side_in[:, slot].reshape(sp_size * side_rows, positions) for slot in slots)
+        )
+        running_row = sum(short_dot(term, upto) for term in side)
+        columns = sum(short_dot(down, term, ((1,), (1,))) for term in side)
         parts = []
         for b in range(sp_size):
             line = b * side_rows
@@ -791,7 +844,6 @@
     units = 2 * sequences
     slots = sequences + 1
     vmem = pl.BlockSpec(memory_space=pltpu.VMEM)
-    smem = pl.BlockSpec(memory_space=pltpu.SMEM)
     anywhere = pl.BlockSpec(memory_space=pl.ANY)
     dma = pltpu.SemaphoreType.DMA
     held = (sp_size, sequences, positions)
@@ -801,9 +853,11 @@
             pltpu.VMEM((sequences, local_heads, share, key_width), jnp.bfloat16),
             pltpu.VMEM((sequences, local_heads, share), jnp.bfloat16),
         ),
-        in_specs=[smem, smem] + [anywhere] * 9,
+        in_specs=[anywhere] * 11,
         out_specs=(vmem, vmem),
         scratch_shapes=[
+            pltpu.SMEM(head_decay_rate.shape, jnp.float32),
+            pltpu.SMEM(next_write_strength.shape, jnp.float32),
             pltpu.VMEM((tp_size, sequences, positions, depth), jnp.bfloat16),
             pltpu.VMEM(key_matrix.shape, jnp.bfloat16),
             pltpu.VMEM(value_matrix.shape, jnp.bfloat16),
@@ -827,7 +881,7 @@
             pltpu.VMEM((sp_size, sequences, 8, value_width), jnp.float32),
             pltpu.VMEM((sp_size, sequences, 8, value_width), jnp.float32),
             dma((sequences,)),
-            dma((8,)),
+            dma((10,)),
             dma((tp_size, units)),
             dma((tp_size, units, 3)),
             dma((3, slots, sp_size)),

time: 38.5 us -> 36.4 us (0.945)
  Pallas kernels: 37.7 us -> 35.7 us
    pallas_call x1, Pallas kernels: 37.1 us -> 35 us  [local_fused(): pl.pallas_call(functools.partial(fused_kernel, sp_size, tp_size), out_sha...]
where the time goes in v3:
time: 36.4 us; the launch traced here: 36.3 us
  Pallas kernels  35.7 us (98%)
  between operations  0.64 us (2%)
    pallas_call x1, Pallas kernels, local_fused(): pl.pallas_call(functools.partial(fused_kernel, sp_size, tp_size), out_sha...  35 us

profile of v3, /device:TPU:0, one launch (start us, length us, event | category | flops | bytes accessed | tf_op | source)
XLA Modules:
  0.0 36.3 jit_solution(6894285108147987299)
XLA Ops:
  0.6 35.0 %shard_map.122 = (bf16[2,4,32,128]{3,2,1,0:T(8,128)(2,1)S(1)}, bf16[2,4,32]{2,1,0:T(4,128)(2,1)S(1)}) custom-call(f32[4]{0:T(128)} %rate_hbm.1, f32[2,4]{1,0:T(2,128)} %next_strength_hbm.1, bf16[2,128,512]{2,1,0:T(8,128)(2,1)} %tokens_ref.1, bf16[4096,512]{1,0:T(8,128)(2,1)} %key_ref.1, bf16[4096,512]{1,0:T(8,128)(2,1)} %value_ref.1, ...), custom_call_target="tpu_custom_call" | custom-call | tf_op jit(solution)/shard_map/pallas_call | solution.py:850
  35.6 0.7 %shard_map.123 = (bf16[2,4,32,128]{3,2,1,0:T(8,128)(2,1)}, bf16[2,4,32]{2,1,0:T(4,128)(2,1)}) custom-call(bf16[2,4,32,128]{3,2,1,0:T(8,128)(2,1)S(1)} %get-tuple-element.6.state_ref, bf16[2,4,32]{2,1,0:T(4,128)(2,1)S(1)} %get-tuple-element.7.read_ref), custom_call_target="tpu_custom_call" | custom-call | tf_op jit(solution)/shard_map/pallas_call | solution.py:910

commit v4 on v3

--- a/solution.py
+++ b/solution.py
@@ -297,7 +297,11 @@
     others = [sp_size - 1 - me, me + 1 - 2 * (me % 2), (me + 2) % sp_size]
 
     loads = [
-        pltpu.make_async_copy(tokens_ref.at[s], gathered.at[spot, s], load_sem.at[s])
+        pltpu.make_async_copy(
+            tokens_ref.at[s],
+            gathered.at[spot, pl.ds(s * positions, positions)],
+            load_sem.at[s],
+        )
         for s in range(sequences)
     ]
     for load in loads:
@@ -342,17 +346,29 @@
         def _(other=other):
             pl.semaphore_signal(peers_sem, inc=1, device_id={"sp": other}, device_id_type=MESH)
 
-    def piece(origin, u, way, target):
+    def crossing(block, send, recv, axis, target):
+        return pltpu.make_async_remote_copy(
+            src_ref=block[0],
+            dst_ref=block[1],
+            send_sem=send,
+            recv_sem=recv,
+            device_id={axis: target},
+            device_id_type=MESH,
+        )
+
+    def piece(origin, u, way, target, own=False):
         s, low, count = units[u]
-        block = gathered.at[origin, s, pl.ds(low, count)]
-        return pltpu.make_async_remote_copy(
-            src_ref=block,
-            dst_ref=block,
-            send_sem=gather_send.at[origin, u, way],
-            recv_sem=gather_recv.at[origin, u],
-            device_id={"tp": target},
-            device_id_type=MESH,
-        )
+        block = gathered.at[origin, pl.ds(s * positions + low, count)]
+        kind = 2 * way + (u == last_unit) + (way == 2 and u == last_unit and own)
+        return crossing(
+            (block, block), gather_send.at[kind], gather_recv.at[origin, u], "tp", target
+        )
+
+    def settle(kind, blocks, count):
+        block = gathered.at[pl.ds(0, blocks), pl.ds(0, count)]
+        crossing(
+            (block, block), gather_send.at[kind], gather_recv.at[0, 0], "tp", partner
+        ).wait_send()
 
     for load in loads:
         load.wait()
@@ -367,7 +383,7 @@
             piece(spot, u, 1, spot - CORES).start()
 
     for u in [last_unit, *range(last_unit)]:
-        piece(spot, u, 2, partner).start()
+        piece(spot, u, 2, partner, own=True).start()
 
     @pl.when(chip < chips - 1)
     def _():
@@ -417,14 +433,20 @@
     def take_one(block, batch):
         s, low, count, _ = batches[batch]
         span = pl.ds(pl.multiple_of(block * depth, depth), depth)
-        add_in(gathered[block, s, low : low + count], span, batch)
+        add_in(gathered[block, s * positions + low : s * positions + low + count], span, batch)
 
     def take_chip(origin_chip, batch):
         s, low, count, _ = batches[batch]
         width = CORES * depth
         span = pl.ds(pl.multiple_of(origin_chip * width, width), width)
         rows = jnp.concatenate(
-            [gathered[origin_chip * CORES + c, s, low : low + count] for c in range(CORES)], axis=1
+            [
+                gathered[
+                    origin_chip * CORES + c, s * positions + low : s * positions + low + count
+                ]
+                for c in range(CORES)
+            ],
+            axis=1,
         )
         add_in(rows, span, batch)
 
@@ -533,22 +555,22 @@
 
         both_sides(distance, act)
 
-    def swap(n, slot, target, origin):
+    def swap(n, slot, target):
         s, low, count, _ = batches[slot]
         if n == 0:
-            source, sink = side_out.at[target, slot], side_in.at[origin, slot]
+            block = side_out.at[target, slot], side_in.at[me, slot]
         else:
             source, sink = ((key_out, key_in), (value_out, value_in))[n - 1]
-            source = source.at[target, s, pl.ds(low, count)]
-            sink = sink.at[origin, s, pl.ds(low, count)]
-        return pltpu.make_async_remote_copy(
-            src_ref=source,
-            dst_ref=sink,
-            send_sem=swap_send.at[n, slot, target],
-            recv_sem=swap_recv.at[n, slot, origin],
-            device_id={"sp": target},
-            device_id_type=MESH,
-        )
+            block = source.at[target, s, pl.ds(low, count)], sink.at[me, s, pl.ds(low, count)]
+        return crossing(block, swap_send.at[n], swap_recv.at[n, s], "sp", target)
+
+    def swapped(n, s):
+        if n == 0:
+            held = sum(batch[0] == s for batch in batches)
+            block = side_in.at[pl.ds(0, sp_size - 1), pl.ds(s, held)]
+        else:
+            block = (key_in, value_in)[n - 1].at[pl.ds(0, sp_size - 1), s]
+        crossing((block, block), swap_send.at[n], swap_recv.at[n, s], "sp", others[0]).wait_recv()
 
     def hand_out(slot):
         s, low, count, _ = batches[slot]
@@ -563,19 +585,19 @@
                 gates[local_heads + h : local_heads + h + 1] - strength_offset
             )
         for other in others:
-            swap(0, slot, other, me).start()
+            swap(0, slot, other).start()
         for h in range(local_heads):
             key_out[h, s, low : low + count] = key_acc[
                 cut, h * key_width : (h + 1) * key_width
             ].astype(jnp.bfloat16)
         for other in others:
-            swap(1, slot, other, me).start()
+            swap(1, slot, other).start()
         for h in range(local_heads):
             value_out[h, s, low : low + count] = value_acc[
                 cut, h * value_width : (h + 1) * value_width
             ].astype(jnp.bfloat16)
         for other in others:
-            swap(2, slot, other, me).start()
+            swap(2, slot, other).start()
         side_in[me, slot] = side_out[me, slot]
         key_in[me, s, low : low + count] = key_out[me, s, low : low + count]
         value_in[me, s, low : low + count] = value_out[me, s, low : low + count]
@@ -638,31 +660,25 @@
         absorb_last_lane(far, lane)
     hand_out(2)
 
-    def settle(u, lane):
-        last = u == last_unit
-        for distance in range(chips):
-            for way, step in ((0, -1), (1, 1)):
-                origin_chip = chip + step * distance
-                origin = origin_chip * CORES + lane
-                onward = chip - step
-                present = (origin_chip >= 0) & (origin_chip < chips)
-                sends = present & (onward >= 0) & (onward < chips)
-
-                if distance or (way == 0 and not last):
-
-                    @pl.when(present & (core == hub(chip)) if last else present)
-                    def _(origin=origin):
-                        piece(origin, u, 2, partner).wait_send()
-
-                @pl.when(sends & (core == 1) if last else sends)
-                def _(origin=origin, way=way, onward=onward):
-                    piece(origin, u, way, onward * CORES + core).wait_send()
-
-    for u in range(last_unit):
-        settle(u, core)
-    piece(spot, last_unit, 2, partner).wait_send()
-    for lane in range(CORES):
-        settle(last_unit, lane)
+    whole, part = last_unit * half, half
+    settle(4, chips, whole)
+    settle(6, 1, part)
+
+    @pl.when(core == hub(chip))
+    def _():
+        settle(5, CORES * far, part)
+
+    for c in range(chips):
+        for way, sent in ((0, c + 1), (1, chips - c)):
+            if sent < chips:
+
+                @pl.when(chip == c)
+                def _(way=way, sent=sent):
+                    settle(2 * way, sent, whole)
+
+                @pl.when((chip == c) & (core == 1))
+                def _(way=way, sent=sent):
+                    settle(2 * way + 1, CORES * sent, part)
 
     side_rows = side_in.shape[2]
     upto = grid_mask(positions, positions, lambda r, c: r <= c).astype(jnp.float32)
@@ -684,12 +700,8 @@
         eye = grid_mask(count, count, lambda r, c: r == c).astype(jnp.float32)
         lower = grid_mask(count, count, lambda r, c: r >= c)
         strict = grid_mask(count, count, lambda r, c: r > c)
-        for slot in slots:
-            for other in others:
-                swap(0, slot, other, other).wait_recv()
-        for slot in slots:
-            for other in others:
-                swap(1, slot, other, other).wait_recv()
+        swapped(0, s)
+        swapped(1, s)
         side = three_terms(
             sum(side_in[:, slot].reshape(sp_size * side_rows, positions) for slot in slots)
         )
@@ -722,9 +734,7 @@
                 else:
                     part[0] = part[0] + short_dot(part[1], part[0])
             covered = covered * 2
-        for slot in slots:
-            for other in others:
-                swap(2, slot, other, other).wait_recv()
+        swapped(2, s)
         solved = []
         for b, part in enumerate(parts):
             values = value_in[b, s].astype(jnp.float32) * part[2]
@@ -735,19 +745,12 @@
             maps.append((both[:, :key_width], both[:, key_width:], part[5]))
         return maps
 
-    def final(n, s, target, origin):
-        source, sink = (
-            (state_out.at[target, s], state_ref.at[s, origin]),
-            (row_out.at[target, s], row_in.at[origin, s]),
+    def final(n, s, target):
+        block = (
+            (state_out.at[target, s], state_ref.at[s, me]),
+            (row_out.at[target, s], row_in.at[me, s]),
         )[n]
-        return pltpu.make_async_remote_copy(
-            src_ref=source,
-            dst_ref=sink,
-            send_sem=last_send.at[n, s, target],
-            recv_sem=last_recv.at[n, s, origin],
-            device_id={"sp": target},
-            device_id_type=MESH,
-        )
+        return crossing(block, last_send.at[n], last_recv.at[n], "sp", target)
 
     def finish(s, maps):
         while len(maps) > 2:
@@ -770,7 +773,7 @@
         for j in range(sp_size):
             state_out[j, s] = turned[j * share : (j + 1) * share, :]
         for other in others:
-            final(0, s, other, me).start()
+            final(0, s, other).start()
         query_read, key_read = reads[0:1], reads[1:2]
         new_value = jnp.sum(side_in[:, s, 2, :], axis=0, keepdims=True)
         raw = query_read + (next_strength_ref[s, me] * meets[s : s + 1]) * (new_value - key_read)
@@ -781,7 +784,7 @@
                 jnp.concatenate([raw[:, turn:], raw[:, :turn]], axis=1) if j else raw
             )
         for other in others:
-            final(1, s, other, me).start()
+            final(1, s, other).start()
         state_ref[s, me] = state_out[me, s]
         row_in[me, s] = row_out[me, s]
 
@@ -789,22 +792,20 @@
     finish(0, block_maps(0, (0,)))
     finish(1, block_maps(1, (1, 2)))
 
-    for slot in range(len(batches)):
-        for n in range(3):
-            for other in others:
-                swap(n, slot, other, me).wait_send()
+    peers = pl.ds(0, sp_size - 1)
+    for n, sent in enumerate((side_out, key_out, value_out)):
+        block = sent.at[peers]
+        crossing((block, block), swap_send.at[n], swap_recv.at[n, 0], "sp", others[0]).wait_send()
+    for n, sent in enumerate((state_out, row_out)):
+        block = sent.at[peers]
+        crossing((block, block), last_send.at[n], last_recv.at[n], "sp", others[0]).wait_send()
+    block = row_in.at[peers]
+    crossing((block, block), last_send.at[1], last_recv.at[1], "sp", others[0]).wait_recv()
     for s in range(sequences):
-        for n in range(2):
-            for other in others:
-                final(n, s, other, me).wait_send()
-    for s in range(sequences):
-        for other in others:
-            final(1, s, other, other).wait_recv()
         rows = jnp.concatenate([row_in[i, s, 0:1, :share] for i in range(sp_size)], axis=0)
         read_ref[s] = (rows * gain_ref[...].reshape(1, share)).astype(jnp.bfloat16)
-    for s in range(sequences):
-        for other in others:
-            final(0, s, other, other).wait_recv()
+    block = state_ref.at[:, peers]
+    crossing((block, block), last_send.at[0], last_recv.at[0], "sp", others[0]).wait_recv()
 
 
 def place_kernel(state_ref, read_ref, state_hbm, read_hbm, sem):
@@ -858,7 +859,7 @@
         scratch_shapes=[
             pltpu.SMEM(head_decay_rate.shape, jnp.float32),
             pltpu.SMEM(next_write_strength.shape, jnp.float32),
-            pltpu.VMEM((tp_size, sequences, positions, depth), jnp.bfloat16),
+            pltpu.VMEM((tp_size, rows, depth), jnp.bfloat16),
             pltpu.VMEM(key_matrix.shape, jnp.bfloat16),
             pltpu.VMEM(value_matrix.shape, jnp.bfloat16),
             pltpu.VMEM(gate_matrix.shape[::-1], jnp.bfloat16),
@@ -883,11 +884,11 @@
             dma((sequences,)),
             dma((10,)),
             dma((tp_size, units)),
-            dma((tp_size, units, 3)),
-            dma((3, slots, sp_size)),
-            dma((3, slots, sp_size)),
-            dma((2, sequences, sp_size)),
-            dma((2, sequences, sp_size)),
+            dma((7,)),
+            dma((3, sequences)),
+            dma((3,)),
+            dma((2,)),
+            dma((2,)),
             pltpu.SemaphoreType.REGULAR,
             pltpu.SemaphoreType.REGULAR,
         ],

time: 36.4 us -> 34.8 us (0.956)
  Pallas kernels: 35.7 us -> 34 us
    pallas_call x1, Pallas kernels: 35 us -> 33.4 us  [local_fused(): pl.pallas_call(functools.partial(fused_kernel, sp_size, tp_size), out_sha...]
where the time goes in v4:
time: 34.8 us; the launch traced here: 34.7 us
  Pallas kernels  34 us (98%)
  between operations  0.64 us (2%)
    pallas_call x1, Pallas kernels, local_fused(): pl.pallas_call(functools.partial(fused_kernel, sp_size, tp_size), out_sha...  33.4 us

profile of v4, /device:TPU:0, one launch (start us, length us, event | category | flops | bytes accessed | tf_op | source)
XLA Modules:
  0.0 34.7 jit_solution(4460786156619836317)
XLA Ops:
  0.6 33.4 %shard_map.122 = (bf16[2,4,32,128]{3,2,1,0:T(8,128)(2,1)S(1)}, bf16[2,4,32]{2,1,0:T(4,128)(2,1)S(1)}) custom-call(f32[4]{0:T(128)} %rate_hbm.1, f32[2,4]{1,0:T(2,128)} %next_strength_hbm.1, bf16[2,128,512]{2,1,0:T(8,128)(2,1)} %tokens_ref.1, bf16[4096,512]{1,0:T(8,128)(2,1)} %key_ref.1, bf16[4096,512]{1,0:T(8,128)(2,1)} %value_ref.1, ...), custom_call_target="tpu_custom_call" | custom-call | tf_op jit(solution)/shard_map/pallas_call | solution.py:851
  34.0 0.7 %shard_map.123 = (bf16[2,4,32,128]{3,2,1,0:T(8,128)(2,1)}, bf16[2,4,32]{2,1,0:T(4,128)(2,1)}) custom-call(bf16[2,4,32,128]{3,2,1,0:T(8,128)(2,1)S(1)} %get-tuple-element.6.state_ref, bf16[2,4,32]{2,1,0:T(4,128)(2,1)S(1)} %get-tuple-element.7.read_ref), custom_call_target="tpu_custom_call" | custom-call | tf_op jit(solution)/shard_map/pallas_call | solution.py:911

commit v5 on v4

--- a/solution.py
+++ b/solution.py
@@ -198,6 +198,13 @@
     second = rest.astype(jnp.bfloat16)
     third = (rest - second.astype(jnp.float32)).astype(jnp.bfloat16)
     return first, second, third
+
+
+def close_dot(left, right):
+    left, right = three_terms(left)[:2], three_terms(right)[:2]
+    return (
+        short_dot(left[0], right[0]) + short_dot(left[0], right[1]) + short_dot(left[1], right[0])
+    )
 
 
 def softplus(x):
@@ -682,46 +689,39 @@
 
     side_rows = side_in.shape[2]
     upto = grid_mask(positions, positions, lambda r, c: r <= c).astype(jnp.float32)
-    down = jnp.concatenate(
-        [
-            grid_mask(positions, positions, lambda r, c: c <= r).astype(jnp.float32),
-            grid_mask(positions, positions, lambda r, c: c == r).astype(jnp.float32),
-        ],
-        axis=0,
-    )
+    down = grid_mask(positions, positions, lambda r, c: c <= r).astype(jnp.float32)
     lanes = pl.ds(pl.multiple_of(me * key_width, key_width), key_width)
     queries = query_ref[:, lanes].astype(jnp.float32)
     new_keys = new_key_ref[:, lanes].astype(jnp.float32)
     new_keys = new_keys * lax.rsqrt(jnp.sum(new_keys * new_keys, axis=-1, keepdims=True) + 1e-06)
     meets = jnp.sum(queries * new_keys, axis=-1, keepdims=True)
+    weight_of_new = [next_strength_ref[s, me] * meets[s : s + 1] for s in range(sequences)]
+    probes = [queries[s : s + 1] - weight_of_new[s] * new_keys[s : s + 1] for s in range(sequences)]
 
     def block_maps(s, slots):
         count = positions
         eye = grid_mask(count, count, lambda r, c: r == c).astype(jnp.float32)
-        lower = grid_mask(count, count, lambda r, c: r >= c)
         strict = grid_mask(count, count, lambda r, c: r > c)
         swapped(0, s)
         swapped(1, s)
-        side = three_terms(
-            sum(side_in[:, slot].reshape(sp_size * side_rows, positions) for slot in slots)
-        )
-        running_row = sum(short_dot(term, upto) for term in side)
-        columns = sum(short_dot(down, term, ((1,), (1,))) for term in side)
+        side = sum(side_in[:, slot].reshape(sp_size * side_rows, positions) for slot in slots)
+        terms = three_terms(side)
+        rows = sum(short_dot(term, upto) for term in terms)
+        columns = sum(short_dot(down, term, ((1,), (1,))) for term in terms)
         parts = []
         for b in range(sp_size):
             line = b * side_rows
-            row = running_row[line : line + 1, :]
-            col = columns[:positions, line : line + 1]
-            strength = columns[positions:, line + 1 : line + 2]
+            row = rows[line : line + 1, :]
+            strength = side[line + 1 : line + 2, :]
+            col = jnp.broadcast_to(columns[:, line : line + 1], (count, count))
             final_log = row[:, count - 1 : count]
             keys = key_in[b, s].astype(jnp.float32)
             keys = keys * lax.rsqrt(jnp.sum(keys * keys, axis=-1, keepdims=True) + 1e-06)
-            within = jnp.where(lower, jnp.exp(jnp.where(lower, col - row, 0.0)), 0.0)
-            scaled = keys * strength
-            power = jnp.where(strict, -short_dot(scaled, keys, ((1,), (1,))) * within, 0.0)
-            erased = scaled * jnp.exp(col)
-            carried = (keys * jnp.exp(final_log - col)).T.astype(jnp.bfloat16)
-            parts.append([eye + power, power, strength, erased, carried, jnp.exp(final_log)])
+            within = jnp.exp(jnp.where(strict, col - row, 0.0)) * -strength
+            power = jnp.where(strict, short_dot(keys, keys, ((1,), (1,))) * within, 0.0)
+            erased = (keys * jnp.exp(col)).astype(jnp.bfloat16)
+            carried = (keys.T * (jnp.exp(final_log - row) * strength)).astype(jnp.bfloat16)
+            parts.append([eye + power, power, erased, carried, jnp.exp(final_log)])
         for part in parts:
             part[1] = short_dot(part[1], part[1])
         covered = 2
@@ -737,12 +737,12 @@
         swapped(2, s)
         solved = []
         for b, part in enumerate(parts):
-            values = value_in[b, s].astype(jnp.float32) * part[2]
-            solved.append(short_dot(part[0], jnp.concatenate([part[3], values], axis=1)))
+            sources = jnp.concatenate([part[2], value_in[b, s]], axis=1)
+            solved.append(short_dot(part[0], sources))
         maps = []
         for part, both in zip(parts, solved):
-            both = short_dot(part[4], both)
-            maps.append((both[:, :key_width], both[:, key_width:], part[5]))
+            both = short_dot(part[3], both)
+            maps.append((both[:, :key_width], both[:, key_width:], part[4]))
         return maps
 
     def final(n, s, target):
@@ -755,28 +755,19 @@
     def finish(s, maps):
         while len(maps) > 2:
             maps = [compose(maps[i + 1], maps[i]) for i in range(0, len(maps), 2)]
-        state = compose_write(maps[1], maps[0][1])
-        wide = (8, key_width)
-        first_row = grid_mask(*wide, lambda r, c: r == 0)
-        probes = jnp.where(
-            first_row,
-            jnp.broadcast_to(queries[s : s + 1], wide),
-            jnp.broadcast_to(new_keys[s : s + 1], wide),
-        )
-        probe_terms, state_terms = three_terms(probes)[:2], three_terms(state)[:2]
-        reads = (
-            short_dot(probe_terms[0], state_terms[0])
-            + short_dot(probe_terms[0], state_terms[1])
-            + short_dot(probe_terms[1], state_terms[0])
-        )
+        (_, first_write, _), (late_map, late_write, late_keep) = maps
+        state = compose_write(maps[1], first_write)
+        probe = jnp.broadcast_to(probes[s], (8, key_width))
+        passed = close_dot(probe, jnp.concatenate([late_write, late_map], axis=1))
+        onto_first = late_keep * probe - passed[:, value_width:]
+        raw = close_dot(onto_first, first_write) + passed[:, :value_width]
         turned = state.T.astype(jnp.bfloat16)
         for j in range(sp_size):
             state_out[j, s] = turned[j * share : (j + 1) * share, :]
         for other in others:
             final(0, s, other).start()
-        query_read, key_read = reads[0:1], reads[1:2]
         new_value = jnp.sum(side_in[:, s, 2, :], axis=0, keepdims=True)
-        raw = query_read + (next_strength_ref[s, me] * meets[s : s + 1]) * (new_value - key_read)
+        raw = raw[0:1] + weight_of_new[s] * new_value
         raw = raw * lax.rsqrt(jnp.sum(raw * raw, axis=-1, keepdims=True) / value_width + 1e-06)
         for j in range(sp_size):
             turn = j * share

time: 34.8 us -> 34.4 us (0.989)
  Pallas kernels: 34 us -> 33.6 us
    pallas_call x1, Pallas kernels: 33.4 us -> 33 us  [local_fused(): pl.pallas_call(functools.partial(fused_kernel, sp_size, tp_size), out_sha...]
where the time goes in v5:
time: 34.4 us; the launch traced here: 34.3 us
  Pallas kernels  33.6 us (98%)
  between operations  0.64 us (2%)
    pallas_call x1, Pallas kernels, local_fused(): pl.pallas_call(functools.partial(fused_kernel, sp_size, tp_size), out_sha...  33 us

profile of v5, /device:TPU:0, one launch (start us, length us, event | category | flops | bytes accessed | tf_op | source)
XLA Modules:
  0.0 34.3 jit_solution(12363140938459370009)
XLA Ops:
  0.6 33.0 %shard_map.122 = (bf16[2,4,32,128]{3,2,1,0:T(8,128)(2,1)S(1)}, bf16[2,4,32]{2,1,0:T(4,128)(2,1)S(1)}) custom-call(f32[4]{0:T(128)} %rate_hbm.1, f32[2,4]{1,0:T(2,128)} %next_strength_hbm.1, bf16[2,128,512]{2,1,0:T(8,128)(2,1)} %tokens_ref.1, bf16[4096,512]{1,0:T(8,128)(2,1)} %key_ref.1, bf16[4096,512]{1,0:T(8,128)(2,1)} %value_ref.1, ...), custom_call_target="tpu_custom_call" | custom-call | tf_op jit(solution)/shard_map/pallas_call | solution.py:842
  33.6 0.7 %shard_map.123 = (bf16[2,4,32,128]{3,2,1,0:T(8,128)(2,1)}, bf16[2,4,32]{2,1,0:T(4,128)(2,1)}) custom-call(bf16[2,4,32,128]{3,2,1,0:T(8,128)(2,1)S(1)} %get-tuple-element.6.state_ref, bf16[2,4,32]{2,1,0:T(4,128)(2,1)S(1)} %get-tuple-element.7.read_ref), custom_call_target="tpu_custom_call" | custom-call | tf_op jit(solution)/shard_map/pallas_call | solution.py:902

commit v6 on v5

--- a/solution.py
+++ b/solution.py
@@ -473,7 +473,7 @@
         for s in range(sequences):
             new_value = short_dot(new_value_ref[s], placer.astype(jnp.float32))
             for h in range(local_heads):
-                side_out[h, s, 2:3, :] = new_value[h : h + 1, :]
+                side_out[h, s, 0, 2:3, :] = new_value[h : h + 1, :]
 
     def own(batch):
         for u in batches[batch][3]:
@@ -565,7 +565,11 @@
     def swap(n, slot, target):
         s, low, count, _ = batches[slot]
         if n == 0:
-            block = side_out.at[target, slot], side_in.at[me, slot]
+            block = (
+                (side_out.at[target, s], side_in.at[me, s])
+                if slot == 0
+                else (side_out.at[target, s, slot - 1], side_in.at[me, s, slot - 1])
+            )
         else:
             source, sink = ((key_out, key_in), (value_out, value_in))[n - 1]
             block = source.at[target, s, pl.ds(low, count)], sink.at[me, s, pl.ds(low, count)]
@@ -573,8 +577,7 @@
 
     def swapped(n, s):
         if n == 0:
-            held = sum(batch[0] == s for batch in batches)
-            block = side_in.at[pl.ds(0, sp_size - 1), pl.ds(s, held)]
+            block = side_in.at[pl.ds(0, sp_size - 1), s]
         else:
             block = (key_in, value_in)[n - 1].at[pl.ds(0, sp_size - 1), s]
         crossing((block, block), swap_send.at[n], swap_recv.at[n, s], "sp", others[0]).wait_recv()
@@ -582,13 +585,14 @@
     def hand_out(slot):
         s, low, count, _ = batches[slot]
         cut = slice(s * positions + low, s * positions + low + count)
+        part = max(slot - 1, 0)
         gates = gate_acc[s, :, low : low + count]
         extra = extra_ref[s, :, low : low + count]
         for h in range(local_heads):
-            side_out[h, slot, 0:1, low : low + count] = (
+            side_out[h, s, part, 0:1, low : low + count] = (
                 -rate_ref[h] * softplus(gates[h : h + 1]) + extra[h : h + 1, :]
             )
-            side_out[h, slot, 1:2, low : low + count] = jax.nn.sigmoid(
+            side_out[h, s, part, 1:2, low : low + count] = jax.nn.sigmoid(
                 gates[local_heads + h : local_heads + h + 1] - strength_offset
             )
         for other in others:
@@ -605,7 +609,10 @@
             ].astype(jnp.bfloat16)
         for other in others:
             swap(2, slot, other).start()
-        side_in[me, slot] = side_out[me, slot]
+        if slot == 0:
+            side_in[me, s] = side_out[me, s]
+        else:
+            side_in[me, s, part] = side_out[me, s, part]
         key_in[me, s, low : low + count] = key_out[me, s, low : low + count]
         value_in[me, s, low : low + count] = value_out[me, s, low : low + count]
 
@@ -667,27 +674,7 @@
         absorb_last_lane(far, lane)
     hand_out(2)
 
-    whole, part = last_unit * half, half
-    settle(4, chips, whole)
-    settle(6, 1, part)
-
-    @pl.when(core == hub(chip))
-    def _():
-        settle(5, CORES * far, part)
-
-    for c in range(chips):
-        for way, sent in ((0, c + 1), (1, chips - c)):
-            if sent < chips:
-
-                @pl.when(chip == c)
-                def _(way=way, sent=sent):
-                    settle(2 * way, sent, whole)
-
-                @pl.when((chip == c) & (core == 1))
-                def _(way=way, sent=sent):
-                    settle(2 * way + 1, CORES * sent, part)
-
-    side_rows = side_in.shape[2]
+    side_rows = side_in.shape[3]
     upto = grid_mask(positions, positions, lambda r, c: r <= c).astype(jnp.float32)
     down = grid_mask(positions, positions, lambda r, c: c <= r).astype(jnp.float32)
     lanes = pl.ds(pl.multiple_of(me * key_width, key_width), key_width)
@@ -698,13 +685,16 @@
     weight_of_new = [next_strength_ref[s, me] * meets[s : s + 1] for s in range(sequences)]
     probes = [queries[s : s + 1] - weight_of_new[s] * new_keys[s : s + 1] for s in range(sequences)]
 
-    def block_maps(s, slots):
+    def block_maps(s):
         count = positions
         eye = grid_mask(count, count, lambda r, c: r == c).astype(jnp.float32)
         strict = grid_mask(count, count, lambda r, c: r > c)
         swapped(0, s)
         swapped(1, s)
-        side = sum(side_in[:, slot].reshape(sp_size * side_rows, positions) for slot in slots)
+        side = jnp.concatenate(
+            [side_in[b, s, 0] + side_in[b, s, 1] for b in range(sp_size)], axis=0
+        )
+        new_value = sum(side[b * side_rows + 2 : b * side_rows + 3] for b in range(sp_size))
         terms = three_terms(side)
         rows = sum(short_dot(term, upto) for term in terms)
         columns = sum(short_dot(down, term, ((1,), (1,))) for term in terms)
@@ -743,7 +733,7 @@
         for part, both in zip(parts, solved):
             both = short_dot(part[3], both)
             maps.append((both[:, :key_width], both[:, key_width:], part[4]))
-        return maps
+        return maps, new_value
 
     def final(n, s, target):
         block = (
@@ -752,12 +742,14 @@
         )[n]
         return crossing(block, last_send.at[n], last_recv.at[n], "sp", target)
 
-    def finish(s, maps):
+    def finish(s, maps, new_value):
         while len(maps) > 2:
             maps = [compose(maps[i + 1], maps[i]) for i in range(0, len(maps), 2)]
         (_, first_write, _), (late_map, late_write, late_keep) = maps
         state = compose_write(maps[1], first_write)
-        probe = jnp.broadcast_to(probes[s], (8, key_width))
+        probe = jnp.where(s == 0, probes[0], probes[1])
+        probe = jnp.broadcast_to(probe, (8, key_width))
+        new_weight = jnp.where(s == 0, weight_of_new[0], weight_of_new[1])
         passed = close_dot(probe, jnp.concatenate([late_write, late_map], axis=1))
         onto_first = late_keep * probe - passed[:, value_width:]
         raw = close_dot(onto_first, first_write) + passed[:, :value_width]
@@ -766,8 +758,7 @@
             state_out[j, s] = turned[j * share : (j + 1) * share, :]
         for other in others:
             final(0, s, other).start()
-        new_value = jnp.sum(side_in[:, s, 2, :], axis=0, keepdims=True)
-        raw = raw[0:1] + weight_of_new[s] * new_value
+        raw = raw[0:1] + new_weight * new_value
         raw = raw * lax.rsqrt(jnp.sum(raw * raw, axis=-1, keepdims=True) / value_width + 1e-06)
         for j in range(sp_size):
             turn = j * share
@@ -780,8 +771,32 @@
         row_in[me, s] = row_out[me, s]
 
     row_out[...] = jnp.zeros_like(row_out)
-    finish(0, block_maps(0, (0,)))
-    finish(1, block_maps(1, (1, 2)))
+
+    def solve(s, carry):
+        finish(s, *block_maps(s))
+        return carry
+
+    lax.fori_loop(0, sequences, solve, 0)
+
+    whole, part = last_unit * half, half
+    settle(4, chips, whole)
+    settle(6, 1, part)
+
+    @pl.when(core == hub(chip))
+    def _():
+        settle(5, CORES * far, part)
+
+    for c in range(chips):
+        for way, sent in ((0, c + 1), (1, chips - c)):
+            if sent < chips:
+
+                @pl.when(chip == c)
+                def _(way=way, sent=sent):
+                    settle(2 * way, sent, whole)
+
+                @pl.when((chip == c) & (core == 1))
+                def _(way=way, sent=sent):
+                    settle(2 * way + 1, CORES * sent, part)
 
     peers = pl.ds(0, sp_size - 1)
     for n, sent in enumerate((side_out, key_out, value_out)):
@@ -834,7 +849,6 @@
     share = value_width // sp_size
     rows = sequences * positions
     units = 2 * sequences
-    slots = sequences + 1
     vmem = pl.BlockSpec(memory_space=pltpu.VMEM)
     anywhere = pl.BlockSpec(memory_space=pl.ANY)
     dma = pltpu.SemaphoreType.DMA
@@ -867,8 +881,8 @@
             pltpu.VMEM((*held, key_width), jnp.bfloat16),
             pltpu.VMEM((*held, value_width), jnp.bfloat16),
             pltpu.VMEM((*held, value_width), jnp.bfloat16),
-            pltpu.VMEM((sp_size, slots, 8, positions), jnp.float32),
-            pltpu.VMEM((sp_size, slots, 8, positions), jnp.float32),
+            pltpu.VMEM((sp_size, sequences, 2, 8, positions), jnp.float32),
+            pltpu.VMEM((sp_size, sequences, 2, 8, positions), jnp.float32),
             pltpu.VMEM((sp_size, sequences, share, key_width), jnp.bfloat16),
             pltpu.VMEM((sp_size, sequences, 8, value_width), jnp.float32),
             pltpu.VMEM((sp_size, sequences, 8, value_width), jnp.float32),

time: 34.4 us -> 34.4 us (level)
  no operation moved by 1% of the time
where the time goes in v6:
time: 34.4 us; the launch traced here: 34.2 us
  Pallas kernels  33.6 us (98%)
  between operations  0.64 us (2%)
    pallas_call x1, Pallas kernels, local_fused(): pl.pallas_call(functools.partial(fused_kernel, sp_size, tp_size), out_sha...  32.9 us

profile of v6, /device:TPU:0, one launch (start us, length us, event | category | flops | bytes accessed | tf_op | source)
XLA Modules:
  0.0 34.2 jit_solution(7480511314785791870)
XLA Ops:
  0.6 32.9 %shard_map.122 = (bf16[2,4,32,128]{3,2,1,0:T(8,128)(2,1)S(1)}, bf16[2,4,32]{2,1,0:T(4,128)(2,1)S(1)}) custom-call(f32[4]{0:T(128)} %rate_hbm.1, f32[2,4]{1,0:T(2,128)} %next_strength_hbm.1, bf16[2,128,512]{2,1,0:T(8,128)(2,1)} %tokens_ref.1, bf16[4096,512]{1,0:T(8,128)(2,1)} %key_ref.1, bf16[4096,512]{1,0:T(8,128)(2,1)} %value_ref.1, ...), custom_call_target="tpu_custom_call" | custom-call | tf_op jit(solution)/shard_map/pallas_call | solution.py:856
  33.6 0.7 %shard_map.123 = (bf16[2,4,32,128]{3,2,1,0:T(8,128)(2,1)}, bf16[2,4,32]{2,1,0:T(4,128)(2,1)}) custom-call(bf16[2,4,32,128]{3,2,1,0:T(8,128)(2,1)S(1)} %get-tuple-element.6.state_ref, bf16[2,4,32]{2,1,0:T(4,128)(2,1)S(1)} %get-tuple-element.7.read_ref), custom_call_target="tpu_custom_call" | custom-call | tf_op jit(solution)/shard_map/pallas_call | solution.py:916

commit v7 on v6

--- a/solution.py
+++ b/solution.py
@@ -424,11 +424,14 @@
     gate_acc[...] = jnp.zeros_like(gate_acc)
     side_out[...] = jnp.zeros_like(side_out)
 
-    def add_in(rows, span, batch):
+    def add_in(rows, span, batch, keys=True, values=True):
         s, low, count, parts = batches[batch]
         cut = slice(s * positions + low, s * positions + low + count)
+        if values:
+            value_acc[cut] += jnp.dot(rows, value_w[span, :], preferred_element_type=jnp.float32)
+        if not keys:
+            return
         key_acc[cut] += jnp.dot(rows, key_w[span, :], preferred_element_type=jnp.float32)
-        value_acc[cut] += jnp.dot(rows, value_w[span, :], preferred_element_type=jnp.float32)
         gates = lax.dot_general(
             gate_own[:, span],
             rows,
@@ -437,10 +440,10 @@
         )
         gate_acc[s, :, low : low + count] += gates
 
-    def take_one(block, batch):
+    def take_one(block, batch, **kinds):
         s, low, count, _ = batches[batch]
         span = pl.ds(pl.multiple_of(block * depth, depth), depth)
-        add_in(gathered[block, s * positions + low : s * positions + low + count], span, batch)
+        add_in(gathered[block, s * positions + low : s * positions + low + count], span, batch, **kinds)
 
     def take_chip(origin_chip, batch):
         s, low, count, _ = batches[batch]
@@ -558,7 +561,13 @@
             def _():
                 piece(block, last_unit, 2, partner).wait_recv()
 
-            take_one(block, len(batches) - 1)
+            take_one(block, len(batches) - 1, values=lane < CORES - 1)
+
+        both_sides(distance, act)
+
+    def absorb_last_values(distance):
+        def act(origin_chip):
+            take_one(origin_chip * CORES + CORES - 1, len(batches) - 1, keys=False)
 
         both_sides(distance, act)
 
@@ -582,7 +591,7 @@
             block = (key_in, value_in)[n - 1].at[pl.ds(0, sp_size - 1), s]
         crossing((block, block), swap_send.at[n], swap_recv.at[n, s], "sp", others[0]).wait_recv()
 
-    def hand_out(slot):
+    def hand_out(slot, before_values=None):
         s, low, count, _ = batches[slot]
         cut = slice(s * positions + low, s * positions + low + count)
         part = max(slot - 1, 0)
@@ -603,6 +612,8 @@
             ].astype(jnp.bfloat16)
         for other in others:
             swap(1, slot, other).start()
+        if before_values is not None:
+            before_values()
         for h in range(local_heads):
             value_out[h, s, low : low + count] = value_acc[
                 cut, h * value_width : (h + 1) * value_width
@@ -672,7 +683,7 @@
         absorb(*pending)
     for lane in range(CORES):
         absorb_last_lane(far, lane)
-    hand_out(2)
+    hand_out(2, lambda: absorb_last_values(far))
 
     side_rows = side_in.shape[3]
     upto = grid_mask(positions, positions, lambda r, c: r <= c).astype(jnp.float32)

time: 34.4 us -> 34.3 us (level)
  no operation moved by 1% of the time
where the time goes in v7:
time: 34.3 us; the launch traced here: 34.1 us
  Pallas kernels  33.5 us (98%)
  between operations  0.64 us (2%)
    pallas_call x1, Pallas kernels, local_fused(): pl.pallas_call(functools.partial(fused_kernel, sp_size, tp_size), out_sha...  32.8 us

profile of v7, /device:TPU:0, one launch (start us, length us, event | category | flops | bytes accessed | tf_op | source)
XLA Modules:
  0.0 34.1 jit_solution(11788744756684253675)
XLA Ops:
  0.6 32.8 %shard_map.122 = (bf16[2,4,32,128]{3,2,1,0:T(8,128)(2,1)S(1)}, bf16[2,4,32]{2,1,0:T(4,128)(2,1)S(1)}) custom-call(f32[4]{0:T(128)} %rate_hbm.1, f32[2,4]{1,0:T(2,128)} %next_strength_hbm.1, bf16[2,128,512]{2,1,0:T(8,128)(2,1)} %tokens_ref.1, bf16[4096,512]{1,0:T(8,128)(2,1)} %key_ref.1, bf16[4096,512]{1,0:T(8,128)(2,1)} %value_ref.1, ...), custom_call_target="tpu_custom_call" | custom-call | tf_op jit(solution)/shard_map/pallas_call | solution.py:867
  33.5 0.7 %shard_map.123 = (bf16[2,4,32,128]{3,2,1,0:T(8,128)(2,1)}, bf16[2,4,32]{2,1,0:T(4,128)(2,1)}) custom-call(bf16[2,4,32,128]{3,2,1,0:T(8,128)(2,1)S(1)} %get-tuple-element.6.state_ref, bf16[2,4,32]{2,1,0:T(4,128)(2,1)S(1)} %get-tuple-element.7.read_ref), custom_call_target="tpu_custom_call" | custom-call | tf_op jit(solution)/shard_map/pallas_call | solution.py:927
